TPU v7x, 128 devices: a whole 4x4x4 slice. The times are simulated.
128 devices in a mesh: fs: 16 (over z, y), tp: 8 (over x, core).
Axes of the slice: x: 4, y: 4, z: 4, core: 2. Of those that a mesh axis runs over, the one named last changes fastest.
Arguments:
- layer_input: bfloat16 [12288, 2048], P('fs', 'tp'), may hold values from -6 to 6
- out_cotangent: bfloat16 [12288, 2048], P('fs', 'tp'), may hold values from -6 to 6
- gate_matrix: bfloat16 [2048, 6144], P('fs', 'tp'), may hold values from -0.125 to 0.125
- up_matrix: bfloat16 [2048, 6144], P('fs', 'tp'), may hold values from -0.125 to 0.125
- down_matrix: bfloat16 [6144, 2048], P('tp', 'fs'), may hold values from -0.078125 to 0.078125
Outputs:
- input_grad: bfloat16 [12288, 2048], P('fs', 'tp')
- gate_grad: float32 [2048, 6144], P('fs', 'tp')
- up_grad: float32 [2048, 6144], P('fs', 'tp')
- down_grad: float32 [6144, 2048], P('tp', 'fs')
All inputs are finite; a program needn't handle non-finite values.
Results may differ from a plain program's by a relative error of at most 0.014.
Values may be sent and summed in bfloat16 or wider, within the bound.
A program may use at most 128 MiB of HBM per device.

v0:
```python
import jax
import jax.numpy as jnp
from jax import lax
from jax.sharding import Mesh
from jax.sharding import PartitionSpec as P

FS = ("fs_0", "fs_1")


def side_by_side(arrays, axis, dim, along):
    both = jnp.concatenate(arrays, axis=along)
    filled, at, done = (lax.all_gather(both, axis, axis=dim, tiled=True), 0, [])
    for a in arrays:
        done.append(lax.slice_in_dim(filled, at, at + a.shape[along], axis=along))
        at += a.shape[along]
    return tuple(done)


def gather_axes(shard, axes, dim):
    filled = shard
    for number in range(len(axes) - 1, -1, -1):
        filled = lax.all_gather(filled, axes[number], axis=dim, tiled=True)
    return filled


def in_blocks(shard, dim, devices):
    lengths = shard.shape
    pieces = shard.reshape(*lengths[:dim], devices, lengths[dim] // devices, *lengths[dim + 1 :])
    return jnp.moveaxis(pieces, dim, 0)


def summed_on_arrival(shard, axis, dim):
    pieces = in_blocks(shard, dim, lax.axis_size(axis))
    arrived = lax.all_to_all(pieces, axis, split_axis=0, concat_axis=0, tiled=True)
    return arrived.astype(jnp.float32).sum(axis=0)


def inner_rows(left, right):
    return lax.dot_general(
        left, right, (((0,), (0,)), ((), ())), preferred_element_type=jnp.float32
    )


def outer_cols(left, right):
    return lax.dot_general(
        left, right, (((1,), (1,)), ((), ())), preferred_element_type=jnp.float32
    )


def on_device(layer_input, out_cotangent, gate_matrix, up_matrix, down_matrix):
    whole_input, whole_cotangent = side_by_side((layer_input, out_cotangent), "tp", 1, 0)
    hidden_cols = gate_matrix.shape[1]
    gate_rows, up_rows = side_by_side((gate_matrix, up_matrix), FS, 0, 1)
    gate_pre = jnp.dot(whole_input, gate_rows, preferred_element_type=jnp.float32)
    up_pre = jnp.dot(whole_input, up_rows, preferred_element_type=jnp.float32)
    hidden_delta = outer_cols(whole_cotangent, gather_axes(down_matrix, FS, 1))
    sigmoid_gate = jax.nn.sigmoid(gate_pre)
    activation = gate_pre * sigmoid_gate
    hidden = (activation * up_pre).astype(jnp.bfloat16)
    up_delta = (hidden_delta * activation).astype(jnp.bfloat16)
    gate_delta = (
        hidden_delta * up_pre * sigmoid_gate * (1.0 + gate_pre * (1.0 - sigmoid_gate))
    ).astype(jnp.bfloat16)
    both_delta = jnp.concatenate((gate_delta, up_delta), axis=1)
    stacked = lax.psum_scatter(
        jnp.concatenate(
            (inner_rows(whole_input, both_delta), inner_rows(whole_cotangent, hidden)), axis=1
        ).astype(jnp.bfloat16),
        FS,
        scatter_dimension=0,
        tiled=True,
    ).astype(jnp.float32)
    gate_grad = stacked[:, :hidden_cols]
    up_grad = stacked[:, hidden_cols : 2 * hidden_cols]
    down_grad = stacked[:, 2 * hidden_cols :].T
    partial_value = outer_cols(gate_delta, gate_rows) + outer_cols(up_delta, up_rows)
    input_grad = summed_on_arrival(partial_value.astype(jnp.bfloat16), "tp", 1).astype(jnp.bfloat16)
    return (input_grad, gate_grad, up_grad, down_grad)


def solution(mesh):
    finer = Mesh(mesh.devices.reshape(4, 4, mesh.shape["tp"]), ("fs_0", "fs_1", "tp"))
    in_specs = (P(FS, "tp"), P(FS, "tp"), P(FS, "tp"), P(FS, "tp"), P("tp", FS))
    out_specs = (P(FS, "tp"), P(FS, "tp"), P(FS, "tp"), P("tp", FS))
    return jax.shard_map(
        on_device, mesh=finer, in_specs=in_specs, out_specs=out_specs, check_vma=False
    )
```

profile of v0, /device:TPU:0, one launch (start us, length us, event | category | flops | bytes accessed | tf_op | source)
XLA Modules:
  0.0 302.3 jit_solution(293238630906716998)
XLA Ops:
  7.2 0.0 copy-start
  7.2 0.0 all-gather.4.cloned.1.call-start
  7.2 2.1 pad_maximum_fusion.1
  9.3 0.0 all-gather.4.cloned.1.call-update
  9.3 0.0 all-gather.8.cloned.1.call-start
  9.4 1.8 pad_maximum_fusion.2
  11.2 0.0 all-gather.8.cloned.1.call-update
  11.2 0.0 all-gather.6.cloned.1.call-start
  11.2 0.0 copy-done
  11.2 18.2 %all_gather.13 = bf16[768,512]{1,0:T(8,128)(2,1)} all-gather(bf16[768,128]{1,0:T(8,128)(2,1)S(1)} %copy-done), channel_id=1, replica_groups=mesh['fs_0'=4,'fs_1'=4,'tp'=8] {'fs_1'}, dimensions={1}, use_global_device_ids=true | all-gather | bytes 983040 | tf_op jit(solution)/shard_map/all_gather | solution.py:22
  29.5 0.0 all-gather.6.cloned.1.call-update
  29.5 0.0 reduce-scatter.4.cloned.1.call-start
  29.6 27.0 %all-gather.4.cloned.1.call-done = bf16[1536,2048]{1,0:T(8,128)(2,1)} async-done(((bf16[1536,256]{1,0:T(8,128)(2,1)}), bf16[1536,2048]{1,0:T(8,128)(2,1)}) %all-gather.4.cloned.1.call-update) | async-done | bytes 6291472 | tf_op jit(solution)/shard_map/all_gather | solution.py:12
  56.6 65.1 %all-gather.8.cloned.1.call-done = bf16[2048,1536]{1,0:T(8,128)(2,1)} async-done(((bf16[128,1536]{1,0:T(8,128)(2,1)}), bf16[2048,1536]{1,0:T(8,128)(2,1)}) %all-gather.8.cloned.1.call-update) | async-done | bytes 6291472 | tf_op jit(solution)/shard_map/all_gather | solution.py:12
  121.7 5.8 %fusion.2 = f32[768,768]{0,1:T(8,128)S(1)} fusion(bf16[2048,1536]{1,0:T(8,128)(2,1)} %all-gather.8.cloned.1.call-done, bf16[1536,2048]{1,0:T(8,128)(2,1)} %all-gather.4.cloned.1.call-done), kind=kOutput, calls=%fused_computation.7 | convolution fusion | flops 2415919104 | bytes 8650752 | tf_op jit(solution)/shard_map/dot_general | solution.py:54
  127.4 0.0 copy-done.1
  127.5 0.7 copy-done.2
  128.1 2.9 fusion.5
  131.0 0.0 copy-done.5
  131.1 0.0 copy-start.6
  131.1 1.5 copy-done.6
  132.5 2.9 convolution_convert_fusion.1
  135.4 27.2 %all-gather.6.cloned.1.call-done = bf16[768,2048]{1,0:T(8,128)(2,1)} async-done(((bf16[768,512]{1,0:T(8,128)(2,1)}), bf16[768,2048]{1,0:T(8,128)(2,1)}) %all-gather.6.cloned.1.call-update) | async-done | bytes 3145744 | tf_op jit(solution)/shard_map/all_gather | solution.py:22
  162.6 7.4 %multiply_convert_fusion.1 = (bf16[768,768]{0,1:T(8,128)(2,1)S(1)}, bf16[768,768]{0,1:T(8,128)(2,1)S(1)}) fusion(f32[768,768]{0,1:T(8,128)} %copy-done.5, f32[768,768]{0,1:T(8,128)} %copy-done.6, bf16[768,2048]{1,0:T(8,128)(2,1)} %all-gather.6.cloned.1.call-done, bf16[1536,2048]{1,0:T(8,128)(2,1)} %all-gather.4.cloned.1.call-done), kind=kOutput, calls=%fused_computation.22 | convolution fusion | flops 2423586816 | bytes 13369344 | tf_op jit(solution)/shard_map/dot_general | solution.py:45
  170.0 0.0 copy-start.3
  170.0 0.0 copy-start.7
  170.0 9.1 %convolution_convert_fusion = bf16[2048,1536]{0,1:T(8,128)(2,1)S(1)} fusion(bf16[1536,2048]{1,0:T(8,128)(2,1)} %all-gather.4.cloned.1.call-done, bf16[768,768]{0,1:T(8,128)(2,1)S(1)} %get-tuple-element.12, bf16[768,768]{0,1:T(8,128)(2,1)S(1)} %get-tuple-element.13), kind=kOutput, calls=%fused_computation.1 | convolution fusion | flops 4839702528 | bytes 11796480 | tf_op jit(solution)/shard_map/dot_general | solution.py:39
  179.1 0.0 copy-done.3
  179.2 0.0 copy-done.7
  179.2 11.4 %pad_maximum_fusion = bf16[2048,2304]{0,1:T(8,128)(2,1)} fusion(bf16[2048,768]{0,1:T(8,128)(2,1)S(1)} %convolution_convert_fusion.1, bf16[2048,1536]{0,1:T(8,128)(2,1)S(1)} %convolution_convert_fusion), kind=kLoop, calls=%fused_computation | loop fusion | flops 18874368 | bytes 18874368 | tf_op jit(solution)/shard_map/concatenate | solution.py:66
  190.6 12.8 %copy.14 = bf16[2048,2304]{1,0:T(8,128)(2,1)} copy(bf16[2048,2304]{0,1:T(8,128)(2,1)} %pad_maximum_fusion) | data formatting | bytes 18874368
  203.4 0.0 reduce-scatter.4.cloned.1.call-update
  203.4 1.2 copy-done.4
  204.7 4.7 %fusion = f32[768,2048]{1,0:T(8,128)S(1)} fusion(bf16[768,768]{0,1:T(8,128)(2,1)S(1)} %copy-done.4, bf16[2048,1536]{1,0:T(8,128)(2,1)} %all-gather.8.cloned.1.call-done), kind=kOutput, calls=%fused_computation.5 | convolution fusion | flops 2415919104 | bytes 10616832 | tf_op jit(solution)/shard_map/dot_general | solution.py:45
  209.4 0.0 slice-done
  209.4 0.0 slice-done.1
  209.4 0.0 copy-done.8
  209.4 3.1 %add_convert_fusion = bf16[768,2048]{1,0:T(8,128)(2,1)S(1)} fusion(f32[768,2048]{1,0:T(8,128)S(1)} %fusion, bf16[768,768]{0,1:T(8,128)(2,1)S(1)} %copy-done.8, bf16[2048,1536]{1,0:T(8,128)(2,1)S(1)} %bitcast.16), kind=kOutput, calls=%fused_computation.2 | convolution fusion | flops 2419064832 | bytes 13762560 | tf_op jit(solution)/shard_map/dot_general | solution.py:45
  212.5 0.2 copy.18
  212.8 42.5 %all_to_all.5 = bf16[8,768,256]{2,1,0:T(8,128)(2,1)S(1)} all-to-all(bf16[8,768,256]{2,1,0:T(8,128)(2,1)S(1)} %bitcast.13), channel_id=1, replica_groups=mesh['fs_0'=4,'fs_1'=4,'tp'=8] {'tp'}, dimensions={0} | all-to-all | bytes 6291456 | tf_op jit(solution)/shard_map/all_to_all | solution.py:34
  255.2 1.3 reduce_sum.12
  256.5 35.1 %reduce-scatter.4.cloned.1.call-done = bf16[128,2304]{1,0:T(8,128)(2,1)} async-done(((bf16[2048,2304]{1,0:T(8,128)(2,1)}), bf16[128,2304]{1,0:T(8,128)(2,1)}) %reduce-scatter.4.cloned.1.call-update) | async-done | bytes 589840
  291.6 1.4 copy.15
  293.0 0.1 fusion.20
  293.1 0.1 convert_element_type.22
  293.1 0.9 copy.13
  294.1 0.9 copy.12
  295.0 0.8 slice_bitcast_fusion
  (8 shorter events, 0.0 us)
Async XLA Ops:
  7.2 4.1 %copy-start = (bf16[768,128]{1,0:T(8,128)(2,1)S(1)}, bf16[768,128]{1,0:T(8,128)(2,1)}, u32[]{:S(2)}) copy-start(bf16[768,128]{1,0:T(8,128)(2,1)} %param.9) | copy-start | bytes 589828
  7.2 49.4 %all-gather.4.cloned.1.call-start = ((), (), s32[]{:S(2)}) async-start(), calls=%async_computation.2 | async-start | bytes 7077888 | tf_op jit(solution)/shard_map/all_gather | solution.py:12
  9.3 112.3 %all-gather.8.cloned.1.call-start = ((), (), s32[]{:S(2)}) async-start(), calls=%async_computation.4 | async-start | bytes 6684672 | tf_op jit(solution)/shard_map/all_gather | solution.py:12
  11.2 151.5 %all-gather.6.cloned.1.call-start = ((), (), s32[]{:S(2)}) async-start(), calls=%async_computation.3 | async-start | bytes 3932160 | tf_op jit(solution)/shard_map/all_gather | solution.py:22
  29.5 262.1 %reduce-scatter.4.cloned.1.call-start = ((), (), s32[]{:S(2)}) async-start(), calls=%async_computation.5 | async-start | bytes 10027008
  121.7 5.8 %copy-start.1 = (bf16[2048,1536]{1,0:T(8,128)(2,1)S(1)}, bf16[2048,1536]{1,0:T(8,128)(2,1)}, u32[]{:S(2)}) copy-start(bf16[2048,1536]{1,0:T(8,128)(2,1)} %all-gather.8.cloned.1.call-done) | copy-start | bytes 18874372
  121.7 6.5 %copy-start.2 = (bf16[1536,2048]{1,0:T(8,128)(2,1)S(1)}, bf16[1536,2048]{1,0:T(8,128)(2,1)}, u32[]{:S(2)}) copy-start(bf16[1536,2048]{1,0:T(8,128)(2,1)} %all-gather.4.cloned.1.call-done) | copy-start | bytes 18874372
  128.1 2.9 copy-start.5
  131.1 1.5 copy-start.6
  170.0 9.1 %copy-start.3 = (bf16[768,768]{0,1:T(8,128)(2,1)}, bf16[768,768]{0,1:T(8,128)(2,1)S(1)}, u32[]{:S(2)}) copy-start(bf16[768,768]{0,1:T(8,128)(2,1)S(1)} %get-tuple-element.13) | copy-start | bytes 3538948
  170.0 9.1 %copy-start.7 = (bf16[768,768]{0,1:T(8,128)(2,1)}, bf16[768,768]{0,1:T(8,128)(2,1)S(1)}, u32[]{:S(2)}) copy-start(bf16[768,768]{0,1:T(8,128)(2,1)S(1)} %get-tuple-element.12) | copy-start | bytes 3538948
  203.4 1.3 copy-start.4
  203.4 6.0 %slice-start = ((s8[6291456]{0:T(1024)(128)(4,1)}), s8[2097152]{0:T(1024)(128)(4,1)S(1)}, s32[]{:S(2)}) async-start(s8[6291456]{0:T(1024)(128)(4,1)} %bitcast.15), calls=%async_computation.6 | async-start | bytes 4194304
  204.7 4.7 %slice-start.1 = ((s8[6291456]{0:T(1024)(128)(4,1)}), s8[4194304]{0:T(1024)(128)(4,1)S(1)}, s32[]{:S(2)}) async-start(s8[6291456]{0:T(1024)(128)(4,1)} %bitcast.15), calls=%async_computation.7 | async-start | bytes 8388608
  204.7 4.7 %copy-start.8 = (bf16[768,768]{0,1:T(8,128)(2,1)S(1)}, bf16[768,768]{0,1:T(8,128)(2,1)}, u32[]{:S(2)}) copy-start(bf16[768,768]{0,1:T(8,128)(2,1)} %copy-done.7) | copy-start | bytes 3538948
Sparse Core Ops, SparseCore 0:
  9.7 46.8 all-gather.3
  59.3 62.3 all-gather.7
  123.3 39.2 all-gather.5
  203.5 88.0 reduce-scatter.3
where the time goes:
time: 303 us; the launch traced here: 302 us
  waiting for transfers between devices  155 us (51%)
  blocking collectives  60.7 us (20%)
  matrix products  35.8 us (12%)
  local copies, waits for them, and re-layouts  20.4 us (7%)
  other arithmetic  16.6 us (5%)
  between operations  13.9 us (5%)
    all_gather x2, waiting for transfers between devices, side_by_side(): filled, at, done = (lax.all_gather(both, axis, axis=dim, tiled=True), 0, [])  92.1 us
    all_to_all x1, blocking collectives, summed_on_arrival(): lax.all_to_all(pieces, axis, split_axis=0, concat_axis=0, tiled=True)  42.5 us
    unnamed x5, waiting for transfers between devices  35.2 us
    all_gather x1, waiting for transfers between devices, gather_axes(): filled = lax.all_gather(filled, axes[number], axis=dim, tiled=True)  27.2 us
    unnamed x26, local copies, waits for them, and re-layouts  19.4 us
    all_gather x1, blocking collectives, gather_axes(): filled = lax.all_gather(filled, axes[number], axis=dim, tiled=True)  18.2 us
    dot_general x3, matrix products, outer_cols(): lax.dot_general(left, right, (((1,), (1,)), ((), ())), preferred_element_...  15.2 us
    dot_general x2, matrix products, inner_rows(): lax.dot_general(left, right, (((0,), (0,)), ((), ())), preferred_element_...  12 us
  transfers between devices with their start and end apart: 4, of which 4 were waited for; matrix products, arithmetic and copies ran while one was open for 7% of the time, Pallas kernels for 0%

commit v1 on v0

v1 whole, which is shorter than its diff:
```python
import jax
import jax.numpy as jnp
from jax import lax
from jax.experimental import pallas as pl
from jax.experimental.pallas import tpu as pltpu
from jax.sharding import PartitionSpec as P

MESH = pl.DeviceIdType.MESH
BF = jnp.bfloat16
F32 = jnp.float32
SIDE = 4
ORDER = (2, 1, -1, 0)


def kernel_of(rows, tokens, width, hidden):
    cols = 3 * hidden // 2
    half = rows // 2
    feats = width // 8
    band = SIDE * rows
    halftok = tokens // 2

    def kernel(x_in, q_in, gate_in, up_in, down_in, dx_out, gate_out, up_out, down_out,
               W, XQ, ACC, D, G, R1, R2, R3, R4, PD, E0, E1, E2, DN, load_sem, ss, rs):
        fs, tp = lax.axis_index("fs"), lax.axis_index("tp")
        z, y = fs // SIDE, fs % SIDE
        x, c = tp // 2, tp % 2

        def turn(a, o):
            return (a + (o % SIDE)) % SIDE

        def fs_dev(f):
            return {"fs": f, "tp": tp}

        def tp_dev(t):
            return {"fs": fs, "tp": t}

        mine = pl.ds(pl.multiple_of(fs * rows, rows), rows)
        my_feats = pl.ds(pl.multiple_of(tp * feats, feats), feats)
        loads = [
            pltpu.make_async_copy(down_in, DN, load_sem.at[0]),
            pltpu.make_async_copy(gate_in, W.at[mine, 0:hidden], load_sem.at[1]),
            pltpu.make_async_copy(up_in, W.at[mine, hidden : 2 * hidden], load_sem.at[2]),
            pltpu.make_async_copy(x_in, XQ.at[0:tokens, my_feats], load_sem.at[3]),
            pltpu.make_async_copy(q_in, XQ.at[tokens : 2 * tokens, my_feats], load_sem.at[4]),
        ]
        for load in loads:
            load.start()

        def big_dev(k, d):
            return fs_dev(turn(z, d) * SIDE + y) if k == 0 else fs_dev(z * SIDE + turn(y, d))

        def small_dev(k, d):
            return big_dev(1 - k, d)

        sibling = tp_dev(x * 2 + (1 - c))

        def x_dev(d):
            return tp_dev(turn(x, d) * 2 + c)

        barrier = pltpu.get_barrier_semaphore()
        for partner in (big_dev(0, 1), big_dev(0, -1), big_dev(1, 1), big_dev(1, -1),
                        x_dev(1), x_dev(-1), sibling):
            pl.semaphore_signal(barrier, inc=1, device_id=partner, device_id_type=MESH)
        loads[0].wait()
        W[mine, 2 * hidden : 3 * hidden] = DN[...].astype(F32).T.astype(BF)
        for load in loads[1:]:
            load.wait()
        pl.semaphore_wait(barrier, 7)

        slots, sent = {}, []

        def slot(name):
            if name not in slots:
                slots[name] = len(slots)
            return slots[name]

        def send(name, src, dst, dev):
            n = slot(name)
            copy = pltpu.make_async_remote_copy(
                src_ref=src, dst_ref=dst, send_sem=ss.at[n], recv_sem=rs.at[n],
                device_id=dev, device_id_type=MESH)
            copy.start()
            sent.append(copy)

        def arrived(name, dst):
            n = slot(name)
            pltpu.make_async_remote_copy(
                src_ref=dst, dst_ref=dst, send_sem=ss.at[n], recv_sem=rs.at[n],
                device_id=sibling, device_id_type=MESH).wait_recv()

        def block(k, so, bo, part=None):
            zo, yo = (bo, so) if k == 0 else (so, bo)
            start = (turn(z, zo) * SIDE + turn(y, yo)) * rows
            if part is None:
                return pl.ds(pl.multiple_of(start, rows), rows)
            return pl.ds(pl.multiple_of(start + part * half, half), half)

        def lanes(k):
            return slice(k * cols, (k + 1) * cols)

        def w(k, so, bo, part=None):
            return W.at[block(k, so, bo, part), lanes(k)]

        def near(k):
            for d in (1, -1):
                send(("a1", k, d), w(k, 0, 0), w(k, 0, 0), small_dev(k, d))

        def far(k, r):
            for d in (1, -1):
                send(("a3", k, r, d), w(k, r, 0), w(k, r, 0), big_dev(k, d))

        def near_arrived(k):
            for d in (1, -1):
                arrived(("a1", k, d), w(k, -d, 0))
                part = 0 if d == 1 else 1
                send(("a2", k, d), w(k, -d, 0, part), w(k, -d, 0, part), small_dev(k, d))

        def opposite_arrived(k):
            for d in (1, -1):
                arrived(("a2", k, d), w(k, 2, 0, 0 if d == 1 else 1))

        def far_arrived(k, r):
            for d in (1, -1):
                arrived(("a3", k, r, d), w(k, r, -d))
                part = 0 if d == 1 else 1
                send(("a4", k, r, d), w(k, r, -d, part), w(k, r, -d, part), big_dev(k, d))

        def last_arrived(k, r):
            for d in (1, -1):
                arrived(("a4", k, r, d), w(k, r, 2, 0 if d == 1 else 1))

        def xq(xo, core, part=None):
            start = (turn(x, xo) * 2 + core) * feats
            lane = pl.ds(pl.multiple_of(start, feats), feats)
            if part is None:
                return XQ.at[:, lane]
            return XQ.at[part * tokens : (part + 1) * tokens, lane]

        near(0)
        near(1)
        for d in (1, -1):
            send(("x1", d), xq(0, c), xq(0, c), x_dev(d))
        far(0, 0)
        far(1, 0)
        send("s0", xq(0, c), xq(0, c), sibling)

        near_arrived(0)
        near_arrived(1)
        for r in (1, -1):
            far(0, r)
            far(1, r)
        far_arrived(0, 0)
        far_arrived(1, 0)
        opposite_arrived(0)
        far(0, 2)
        opposite_arrived(1)
        far(1, 2)

        for d in (1, -1):
            arrived(("x1", d), xq(-d, c))
            part = 0 if d == 1 else 1
            send(("x2", d), xq(-d, c, part), xq(-d, c, part), x_dev(d))
        for d in (1, -1):
            send(("s1", d), xq(-d, c), xq(-d, c), sibling)
        far_arrived(0, 1)
        far_arrived(1, 1)
        for d in (1, -1):
            part = 0 if d == 1 else 1
            arrived(("x2", d), xq(2, c, part))
            send(("s2", d), xq(2, c, part), xq(2, c, part), sibling)
        far_arrived(0, -1)
        far_arrived(1, -1)
        arrived("s0", xq(0, 1 - c))
        for d in (1, -1):
            arrived(("s1", d), xq(-d, 1 - c))
        for d in (1, -1):
            arrived(("s2", d), xq(2, 1 - c, 0 if d == 1 else 1))

        tile = tokens // 3

        def dot(a, b, dims):
            return lax.dot_general(a, b, (dims, ((), ())), preferred_element_type=F32)

        def put(at, lane, value, first):
            if first:
                ACC[at, lane] = value
            else:
                ACC[at, lane] += value

        def forward(k, o, first=False):
            def piece(m, carry):
                at = pl.ds(pl.multiple_of(m * tile, tile), tile)
                low = pl.ds(pl.multiple_of(tokens + m * tile, tile), tile)
                if k == 0:
                    span = pl.ds(pl.multiple_of(turn(z, o) * band, band), band)
                    put(at, slice(0, cols),
                        dot(XQ[at, span], W[span, 0:cols], ((1,), (0,))), first)
                else:
                    spans = [pl.ds(pl.multiple_of(i * band + turn(y, o) * rows, rows), rows)
                             for i in range(SIDE)]
                    a = jnp.concatenate([XQ[at, s] for s in spans], axis=1)
                    b = jnp.concatenate([W[s, cols : 2 * hidden] for s in spans], axis=0)
                    put(at, slice(cols, 2 * hidden), dot(a, b, ((1,), (0,))), first)
                    a = jnp.concatenate([XQ[low, s] for s in spans], axis=1)
                    b = jnp.concatenate([W[s, 2 * hidden : 3 * hidden] for s in spans], axis=0)
                    put(at, slice(2 * hidden, 3 * hidden), dot(a, b, ((1,), (0,))), first)
                return carry
            lax.fori_loop(0, 3, piece, 0)

        forward(0, 0, True)
        forward(1, 0, True)
        far_arrived(0, 2)
        far_arrived(1, 2)
        for o in (1, -1):
            forward(0, o)
            forward(1, o)
        for k in (0, 1):
            for r in (0, 1, -1, 2):
                last_arrived(k, r)
            forward(k, 2)

        step = tokens // 24

        def gate(m, carry):
            at = pl.ds(pl.multiple_of(m * step, step), step)
            g = ACC[at, 0:hidden]
            u = ACC[at, hidden : 2 * hidden]
            e = ACC[at, 2 * hidden : 3 * hidden]
            s = jax.nn.sigmoid(g)
            act = g * s
            D[at, 0:hidden] = (e * u * s * (1.0 + g * (1.0 - s))).astype(BF)
            D[at, hidden : 2 * hidden] = (e * act).astype(BF)
            D[at, 2 * hidden : 3 * hidden] = (act * u).astype(BF)
            return carry

        lax.fori_loop(0, 24, gate, 0)

        def grads(k, o):
            def piece(p, carry):
                if k == 0:
                    span = pl.ds(pl.multiple_of(turn(z, o) * band + p * 2 * rows, 2 * rows), 2 * rows)
                    G[span, 0:cols] = dot(
                        XQ[0:tokens, span], D[:, 0:cols], ((0,), (0,))).astype(BF)
                else:
                    spans = [pl.ds(pl.multiple_of((2 * p + i) * band + turn(y, o) * rows, rows), rows)
                             for i in range(2)]
                    a = jnp.concatenate([XQ[0:tokens, s] for s in spans], axis=1)
                    r = dot(a, D[:, cols : 2 * hidden], ((0,), (0,))).astype(BF)
                    a = jnp.concatenate([XQ[tokens : 2 * tokens, s] for s in spans], axis=1)
                    t = dot(a, D[:, 2 * hidden : 3 * hidden], ((0,), (0,))).astype(BF)
                    for i in range(2):
                        G[spans[i], cols : 2 * hidden] = r[i * rows : (i + 1) * rows]
                        G[spans[i], 2 * hidden : 3 * hidden] = t[i * rows : (i + 1) * rows]
                return carry
            lax.fori_loop(0, 2, piece, 0)

        def g(k, so, bo, part=None):
            return G.at[block(k, so, bo, part), lanes(k)]

        def add_into(ref, *others):
            def piece(m, carry):
                at = pl.ds(pl.multiple_of(m * 16, 16), 16)
                total = ref[at, :].astype(F32)
                for other in others:
                    total = total + other[at, :].astype(F32)
                ref[at, :] = total.astype(BF)
                return carry
            lax.fori_loop(0, ref.shape[0] // 16, piece, 0)

        def s1(k):
            for j, r in enumerate(ORDER):
                for i, d in enumerate((1, -1)):
                    send(("g1", k, j, d), g(k, r, 2, i), R1.at[k, i, j], big_dev(k, d))

        def s2(k, j):
            r = ORDER[j]
            for i, d in enumerate((1, -1)):
                arrived(("g1", k, j, d), R1.at[k, i, j])
                add_into(g(k, r, d, i), R1.at[k, i, j])
            for i, d in enumerate((1, -1)):
                send(("g2", k, j, d), g(k, r, d), R2.at[k, i, j], big_dev(k, d))

        def two(k, j):
            for i, d in enumerate((1, -1)):
                arrived(("g2", k, j, d), R2.at[k, i, j])

        def s3(k):
            two(k, 0)
            add_into(g(k, 2, 0), R2.at[k, 0, 0], R2.at[k, 1, 0])
            for i, d in enumerate((1, -1)):
                send(("g3", k, d), g(k, 2, 0, i), R3.at[k, i], small_dev(k, d))

        def s4(k, i):
            d = (1, -1)[i]
            two(k, 1 + i)
            add_into(g(k, d, 0), R2.at[k, 0, 1 + i], R2.at[k, 1, 1 + i])
            arrived(("g3", k, d), R3.at[k, i])
            add_into(g(k, d, 0, i), R3.at[k, i])
            send(("g4", k, d), g(k, d, 0), R4.at[k, i], small_dev(k, d))

        def partial_of(xo, core):
            start = (turn(x, xo) * 2 + core) * feats
            span = pl.ds(pl.multiple_of(start, feats), feats)

            def piece(m, carry):
                at = pl.ds(pl.multiple_of(m * tile, tile), tile)
                PD[at, span] = dot(
                    D[at, 0 : 2 * hidden], W[span, 0 : 2 * hidden], ((1,), (1,))).astype(BF)
                return carry
            lax.fori_loop(0, 3, piece, 0)

        def pd(xo, core, part=None):
            start = (turn(x, xo) * 2 + core) * feats
            lane = pl.ds(pl.multiple_of(start, feats), feats)
            if part is None:
                return PD.at[:, lane]
            return PD.at[part * halftok : (part + 1) * halftok, lane]

        grads(0, 2)
        s1(0)
        grads(1, 2)
        s1(1)
        for o in (1, -1):
            grads(0, o)
            grads(1, o)
        for j in (0, 1, 2):
            s2(0, j)
            s2(1, j)
        for j, r in enumerate(ORDER):
            partial_of(r, 1 - c)
            send(("d0", j), pd(r, 1 - c), E0.at[j], sibling)
        for r in ORDER:
            partial_of(r, c)
        arrived(("d0", 0), E0.at[0])
        add_into(pd(2, c), E0.at[0])
        for i, d in enumerate((1, -1)):
            send(("d1", d), pd(2, c, i), E1.at[i], x_dev(d))
        grads(0, 0)
        grads(1, 0)
        for j in (1, 2):
            arrived(("d0", j), E0.at[j])
            add_into(pd(ORDER[j], c), E0.at[j])
        s3(0)
        s3(1)
        s2(0, 3)
        s2(1, 3)
        for i, d in enumerate((1, -1)):
            arrived(("d1", d), E1.at[i])
            add_into(pd(d, c, i), E1.at[i])
            send(("d2", d), pd(d, c), E2.at[i], x_dev(d))
        for i in (0, 1):
            s4(0, i)
            s4(1, i)
        arrived(("d0", 3), E0.at[3])
        for i, d in enumerate((1, -1)):
            arrived(("d2", d), E2.at[i])

        own = pd(0, c)

        def last_dx(m, carry):
            at = pl.ds(pl.multiple_of(m * 16, 16), 16)
            total = (own[at, :].astype(F32) + E0[3, at, :].astype(F32)
                     + E2[0, at, :].astype(F32) + E2[1, at, :].astype(F32))
            dx_out[at, :] = total.astype(BF)
            return carry

        lax.fori_loop(0, tokens // 16, last_dx, 0)
        for k in (0, 1):
            two(k, 3)
            for i, d in enumerate((1, -1)):
                arrived(("g4", k, d), R4.at[k, i])
            base = g(k, 0, 0)

            def last_grad(m, carry):
                at = pl.ds(pl.multiple_of(m * 16, 16), 16)
                total = (base[at, :].astype(F32) + R2[k, 0, 3, at, :].astype(F32)
                         + R2[k, 1, 3, at, :].astype(F32) + R4[k, 0, at, :].astype(F32)
                         + R4[k, 1, at, :].astype(F32))
                rest = cols - hidden
                if k == 0:
                    gate_out[at, :] = total[:, 0:hidden]
                    up_out[at, 0:rest] = total[:, hidden:cols]
                else:
                    up_out[at, rest:hidden] = total[:, 0:rest]
                    down_out[at, :] = total[:, rest:cols]
                return carry

            lax.fori_loop(0, rows // 16, last_grad, 0)
        for copy in sent:
            copy.wait_send()

    count = 2 * (2 + 2 + 8 + 8) + 9 + 2 * (8 + 8 + 2 + 2) + 4 + 2 + 2
    scratch = [
        pltpu.VMEM((width, 2 * cols), BF),
        pltpu.VMEM((2 * tokens, width), BF),
        pltpu.VMEM((tokens, 2 * cols), F32),
        pltpu.VMEM((tokens, 2 * cols), BF),
        pltpu.VMEM((width, 2 * cols), BF),
        pltpu.VMEM((2, 2, SIDE, half, cols), BF),
        pltpu.VMEM((2, 2, SIDE, rows, cols), BF),
        pltpu.VMEM((2, 2, half, cols), BF),
        pltpu.VMEM((2, 2, rows, cols), BF),
        pltpu.VMEM((tokens, width), BF),
        pltpu.VMEM((SIDE, tokens, feats), BF),
        pltpu.VMEM((2, halftok, feats), BF),
        pltpu.VMEM((2, tokens, feats), BF),
        pltpu.VMEM((hidden, rows), BF),
        pltpu.SemaphoreType.DMA((5,)),
        pltpu.SemaphoreType.DMA((count,)),
        pltpu.SemaphoreType.DMA((count,)),
    ]
    return kernel, scratch


def solution(mesh):
    def on_device(layer_input, out_cotangent, gate_matrix, up_matrix, down_matrix):
        tokens, feats = layer_input.shape
        rows, hidden = gate_matrix.shape
        width = feats * mesh.shape["tp"]
        kernel, scratch = kernel_of(rows, tokens, width, hidden)
        flops = 2 * 8 * tokens * width * hidden
        dx, gate_grad, up_grad, down_grad = pl.pallas_call(
            kernel,
            out_shape=(
                jax.ShapeDtypeStruct((tokens, feats), BF),
                jax.ShapeDtypeStruct((rows, hidden), F32),
                jax.ShapeDtypeStruct((rows, hidden), F32),
                jax.ShapeDtypeStruct((rows, hidden), F32),
            ),
            in_specs=[pl.BlockSpec(memory_space=pl.ANY)] * 5,
            out_specs=[pl.BlockSpec(memory_space=pltpu.VMEM)] * 4,
            scratch_shapes=scratch,
            compiler_params=pltpu.CompilerParams(
                collective_id=0, has_side_effects=True, vmem_limit_bytes=66_000_000),
            cost_estimate=pl.CostEstimate(
                flops=flops, bytes_accessed=4 << 20, transcendentals=tokens * hidden),
        )(layer_input, out_cotangent, gate_matrix, up_matrix, down_matrix)
        return dx, gate_grad, up_grad, down_grad.T

    return jax.shard_map(
        on_device, mesh=mesh,
        in_specs=(P("fs", "tp"), P("fs", "tp"), P("fs", "tp"), P("fs", "tp"), P("tp", "fs")),
        out_specs=(P("fs", "tp"), P("fs", "tp"), P("fs", "tp"), P("tp", "fs")),
        check_vma=False)
```

time: 303 us -> 122 us (0.40)
  waiting for transfers between devices: 155 us -> 0 us
  Pallas kernels: 0 us -> 116 us
  blocking collectives: 60.7 us -> 0 us
  matrix products: 35.8 us -> 0 us
  other arithmetic: 16.6 us -> 0 us
  local copies, waits for them, and re-layouts: 20.4 us -> 4.98 us
  between operations: 13.9 us -> 0.65 us
    all_gather x3 -> x0, waiting for transfers between devices: 119 us -> none  [the longest x2 92.1 us: side_by_side(): filled, at, done = (lax.all_gather(both, axis, axis=dim, tiled=True), 0, [])]
    pallas_call x0 -> x1, Pallas kernels: none -> 116 us  [on_device(): pl.pallas_call(kernel, out_shape=(jax.ShapeDtypeStruct((tokens, feats), B...]
    all_to_all x1 -> x0, blocking collectives: 42.5 us -> none  [summed_on_arrival(): lax.all_to_all(pieces, axis, split_axis=0, concat_axis=0, tiled=True)]
    dot_general x7 -> x0, matrix products: 35.8 us -> none  [the longest x3 15.2 us: outer_cols(): lax.dot_general(left, right, (((1,), (1,)), ((), ())), preferred_element_...]
    unnamed x5 -> x0, waiting for transfers between devices: 35.2 us -> none
    all_gather x1 -> x0, blocking collectives: 18.2 us -> none  [gather_axes(): filled = lax.all_gather(filled, axes[number], axis=dim, tiled=True)]
    concatenate x3 -> x0, other arithmetic: 15.3 us -> none  [the longest x1 11.4 us: on_device(): jnp.concatenate((inner_rows(whole_input, both_delta), inner_rows(whole_co...]
    unnamed x26 -> x10, local copies, waits for them, and re-layouts: 19.4 us -> 4.98 us
  transfers between devices with their start and end apart: 4 -> 0, of which waited for: 4 -> 0; matrix products, arithmetic and copies ran while one was open for 7% -> 0% of each run, Pallas kernels for 0% -> 0%
where the time goes in v1:
time: 122 us; the launch traced here: 121 us
  Pallas kernels  116 us (95%)
  local copies, waits for them, and re-layouts  4.98 us (4%)
    pallas_call x1, Pallas kernels, on_device(): pl.pallas_call(kernel, out_shape=(jax.ShapeDtypeStruct((tokens, feats), B...  116 us
    unnamed x10, local copies, waits for them, and re-layouts  4.98 us

profile of v1, /device:TPU:0, one launch (start us, length us, event | category | flops | bytes accessed | tf_op | source)
XLA Modules:
  0.0 121.5 jit_solution(15403955666599404806)
XLA Ops:
  0.6 115.8 %shard_map.84 = (bf16[768,256]{1,0:T(8,128)(2,1)}, f32[128,768]{1,0:T(8,128)}, f32[128,768]{1,0:T(8,128)}, f32[128,768]{1,0:T(8,128)}) custom-call(bf16[768,256]{1,0:T(8,128)(2,1)} %x_in.1, bf16[768,256]{1,0:T(8,128)(2,1)} %q_in.1, bf16[128,768]{1,0:T(8,128)(2,1)} %gate_in.1, bf16[128,768]{1,0:T(8,128)(2,1)} %up_in.1, bf16[768,128]{1,0:T(8,128)(2,1)} %down_in.1), custom_call_target="tpu_custom_call" | custom-call | flops 19327352832 | bytes 4194304 | tf_op jit(solution)/shard_map/pallas_call | solution.py:422
  116.5 0.0 copy-start.2
  116.5 2.0 %copy.9 = f32[768,128]{1,0:T(8,128)} copy(f32[768,128]{0,1:T(8,128)} %bitcast.1) | data formatting | bytes 786432
  118.4 0.0 copy-done.2
  118.4 0.0 copy-start.1
  118.4 0.7 copy.13
  119.2 0.4 copy-done.1
  119.6 0.0 copy-start
  119.6 0.7 copy.14
  120.3 0.4 copy-done
  120.7 0.7 copy.15
Async XLA Ops:
  116.5 2.0 %copy-start.2 = (bf16[768,256]{1,0:T(8,128)(2,1)S(1)}, bf16[768,256]{1,0:T(8,128)(2,1)}, u32[]{:S(2)}) copy-start(bf16[768,256]{1,0:T(8,128)(2,1)} %get-tuple-element.20) | copy-start | bytes 1179652
  118.4 1.1 copy-start.1
  119.6 1.1 copy-start

commit v2 on v0

v2 whole, which is shorter than its diff:
```python
import jax
import jax.numpy as jnp
from jax import lax
from jax.experimental import pallas as pl
from jax.experimental.pallas import tpu as pltpu
from jax.sharding import PartitionSpec as P

MESH = pl.DeviceIdType.MESH
BF = jnp.bfloat16
F32 = jnp.float32
SIDE = 4
ORDER = (2, 1, -1, 0)


def shares(hidden):
    first = 2 * hidden // 3
    return (first, hidden - first), (0, 3 * first)


def kernel_of(rows, tokens, width, hidden):
    size, base = shares(hidden)
    half = rows // 2
    feats = width // 8
    band = SIDE * rows
    halftok = tokens // 2
    every = 3 * hidden

    def kernel(x_in, q_in, gate_in, up_in, down_in, dx_out, sum_out, late_out,
               W, XQ, ACC, D, G, R1a, R1b, R2a, R2b, R3a, R3b, R4a, PD, E0, E1, E2, DN, SUM, DX,
               load_sem, store_sem, ss, rs):
        R1, R2, R3, R4 = (R1a, R1b), (R2a, R2b), (R3a, R3b), (R4a, late_out)
        fs, tp = lax.axis_index("fs"), lax.axis_index("tp")
        z, y = fs // SIDE, fs % SIDE
        x, c = tp // 2, tp % 2

        def turn(a, o):
            return (a + (o % SIDE)) % SIDE

        def fs_dev(f):
            return {"fs": f, "tp": tp}

        def tp_dev(t):
            return {"fs": fs, "tp": t}

        def big_dev(k, d):
            return fs_dev(turn(z, d) * SIDE + y) if k == 0 else fs_dev(z * SIDE + turn(y, d))

        def small_dev(k, d):
            return big_dev(1 - k, d)

        sibling = tp_dev(x * 2 + (1 - c))

        def x_dev(d):
            return tp_dev(turn(x, d) * 2 + c)

        barrier = pltpu.get_barrier_semaphore()
        for partner in (big_dev(0, 1), big_dev(0, -1), big_dev(1, 1), big_dev(1, -1),
                        x_dev(1), x_dev(-1), sibling):
            pl.semaphore_signal(barrier, inc=1, device_id=partner, device_id_type=MESH)
        mine = pl.ds(pl.multiple_of(fs * rows, rows), rows)
        my_feats = pl.ds(pl.multiple_of(tp * feats, feats), feats)
        loads = [
            pltpu.make_async_copy(down_in, DN, load_sem.at[0]),
            pltpu.make_async_copy(x_in, XQ.at[0:tokens, my_feats], load_sem.at[1]),
            pltpu.make_async_copy(q_in, XQ.at[tokens : 2 * tokens, my_feats], load_sem.at[2]),
        ]
        for p in (0, 1):
            at, h, from_ = base[p], size[p], p * size[0]
            for i, ref in enumerate((gate_in, up_in)):
                loads.append(pltpu.make_async_copy(
                    ref.at[:, from_ : from_ + h], W.at[mine, at + i * h : at + (i + 1) * h],
                    load_sem.at[len(loads)]))
        for load in loads:
            load.start()

        def load_in():
            loads[0].wait()
            turned = DN[...].astype(F32).T.astype(BF)
            for p in (0, 1):
                at, h, from_ = base[p], size[p], p * size[0]
                W[mine, at + 2 * h : at + 3 * h] = turned[:, from_ : from_ + h]
            for load in loads[1:]:
                load.wait()

        load_in()

        def meet():
            pl.semaphore_wait(barrier, 7)

        meet()

        slots = {}

        def slot(name):
            if name not in slots:
                slots[name] = len(slots)
            return slots[name]

        def send(group, name, src, dst, dev):
            pltpu.make_async_remote_copy(
                src_ref=src, dst_ref=dst, send_sem=ss.at[group], recv_sem=rs.at[slot(name)],
                device_id=dev, device_id_type=MESH).start()

        def awaited(name, like):
            return pltpu.make_async_remote_copy(
                src_ref=like, dst_ref=like, send_sem=ss.at[0], recv_sem=rs.at[slot(name)],
                device_id=sibling, device_id_type=MESH)

        def arrived(name, like):
            awaited(name, like).wait_recv()

        def left(group, like):
            pltpu.make_async_remote_copy(
                src_ref=like, dst_ref=like, send_sem=ss.at[group], recv_sem=rs.at[0],
                device_id=sibling, device_id_type=MESH).wait_send()

        def block(k, so, bo, part=None):
            zo, yo = (bo, so) if k == 0 else (so, bo)
            start = (turn(z, zo) * SIDE + turn(y, yo)) * rows
            if part is None:
                return pl.ds(pl.multiple_of(start, rows), rows)
            return pl.ds(pl.multiple_of(start + part * half, half), half)

        def lanes(p, k):
            cols = 3 * size[p] // 2
            return slice(base[p] + k * cols, base[p] + (k + 1) * cols)

        def blocks(ref, p, n):
            return ref.at[0 : n * rows, base[p] : base[p] + 3 * size[p]]

        def w(p, k, so, bo, part=None):
            return W.at[block(k, so, bo, part), lanes(p, k)]

        def near(p, k):
            for d in (1, -1):
                send(p, ("a1", p), w(p, k, 0, 0), w(p, k, 0, 0), small_dev(k, d))

        def far(p, r):
            for k in (0, 1):
                for d in (1, -1):
                    send(p, ("a3", p, r), w(p, k, r, 0), w(p, k, r, 0), big_dev(k, d))

        def near_arrived(p):
            arrived(("a1", p), blocks(W, p, 2))
            for k in (0, 1):
                for i, d in enumerate((1, -1)):
                    send(p, ("a2", p), w(p, k, -d, 0, i), w(p, k, -d, 0, i), small_dev(k, d))

        def opposite_arrived(p):
            arrived(("a2", p), blocks(W, p, 1))

        def far_arrived(p, r):
            arrived(("a3", p, r), blocks(W, p, 2))
            for k in (0, 1):
                for i, d in enumerate((1, -1)):
                    send(p, ("a4", p), w(p, k, r, -d, i), w(p, k, r, -d, i), big_dev(k, d))

        def last_arrived(p):
            arrived(("a4", p), blocks(W, p, 4))

        def xq(xo, core, part):
            start = (turn(x, xo) * 2 + core) * feats
            lane = pl.ds(pl.multiple_of(start, feats), feats)
            return XQ.at[part * tokens : (part + 1) * tokens, lane]

        def x_own(i):
            for d in (1, -1):
                part = i if d == 1 else 1 - i
                send(2, ("x1", i), xq(0, c, part), xq(0, c, part), x_dev(d))

        def to_sibling(xo, part):
            send(2, "sib", xq(xo, c, part), xq(xo, c, part), sibling)

        def x_first():
            arrived(("x1", 0), XQ.at[:, 0:feats])
            for i, d in enumerate((1, -1)):
                send(2, "x2", xq(-d, c, i), xq(-d, c, i), x_dev(d))
            for i, d in enumerate((1, -1)):
                to_sibling(-d, i)

        def x_second():
            arrived(("x1", 1), XQ.at[:, 0:feats])
            for i, d in enumerate((1, -1)):
                to_sibling(-d, 1 - i)

        def x_third():
            arrived("x2", XQ.at[:, 0:feats])
            for i in (0, 1):
                to_sibling(2, i)

        def x_last():
            arrived("sib", XQ.at[:, 0 : 4 * feats])

        near(0, 0)
        x_own(0)
        near(0, 1)
        far(0, 0)
        x_own(1)
        for part in (0, 1):
            to_sibling(0, part)
        for k in (0, 1):
            near(1, k)

        near_arrived(0)
        for r in (1, -1):
            far(0, r)
        x_first()
        far_arrived(0, 0)
        near_arrived(1)
        opposite_arrived(0)
        far(0, 2)
        far_arrived(0, 1)
        x_second()
        far_arrived(0, -1)
        far(1, 0)
        x_third()
        far_arrived(0, 2)
        for r in (1, -1):
            far(1, r)
        opposite_arrived(1)
        far(1, 2)
        x_last()

        tile = tokens // 3

        def dot(a, b, dims):
            return lax.dot_general(a, b, (dims, ((), ())), preferred_element_type=F32)

        def put(at, lane, value, first):
            if first:
                ACC[at, lane] = value
            else:
                ACC[at, lane] += value

        def forward(p, k, o, first=False):
            both = lanes(p, k)
            split = base[p] + 2 * size[p]

            def piece(m, carry):
                at = pl.ds(pl.multiple_of(m * tile, tile), tile)
                low = pl.ds(pl.multiple_of(tokens + m * tile, tile), tile)
                if k == 0:
                    span = pl.ds(pl.multiple_of(turn(z, o) * band, band), band)
                    put(at, both, dot(XQ[at, span], W[span, both], ((1,), (0,))), first)
                else:
                    spans = [pl.ds(pl.multiple_of(i * band + turn(y, o) * rows, rows), rows)
                             for i in range(SIDE)]
                    for top, lane in ((at, slice(both.start, split)), (low, slice(split, both.stop))):
                        a = jnp.concatenate([XQ[top, s] for s in spans], axis=1)
                        b = jnp.concatenate([W[s, lane] for s in spans], axis=0)
                        put(at, lane, dot(a, b, ((1,), (0,))), first)
                return carry
            lax.fori_loop(0, 3, piece, 0)

        step = tokens // 24

        def gate(p):
            h = size[p]
            one, two, three, four = (base[p] + i * h for i in range(4))

            def piece(m, carry):
                at = pl.ds(pl.multiple_of(m * step, step), step)
                g = ACC[at, one:two]
                u = ACC[at, two:three]
                e = ACC[at, three:four]
                s = jax.nn.sigmoid(g)
                act = g * s
                D[at, one:two] = (e * u * s * (1.0 + g * (1.0 - s))).astype(BF)
                D[at, two:three] = (e * act).astype(BF)
                D[at, three:four] = (act * u).astype(BF)
                return carry

            lax.fori_loop(0, 24, piece, 0)

        def grads(p, k, o):
            both = lanes(p, k)
            split = base[p] + 2 * size[p]

            def piece(n, carry):
                if k == 0:
                    span = pl.ds(pl.multiple_of(turn(z, o) * band + n * 2 * rows, 2 * rows), 2 * rows)
                    G[span, both] = dot(XQ[0:tokens, span], D[:, both], ((0,), (0,))).astype(BF)
                else:
                    spans = [pl.ds(pl.multiple_of((2 * n + i) * band + turn(y, o) * rows, rows), rows)
                             for i in range(2)]
                    for top, lane in ((0, slice(both.start, split)), (tokens, slice(split, both.stop))):
                        a = jnp.concatenate([XQ[top : top + tokens, s] for s in spans], axis=1)
                        r = dot(a, D[:, lane], ((0,), (0,))).astype(BF)
                        for i in range(2):
                            G[spans[i], lane] = r[i * rows : (i + 1) * rows]
                return carry
            lax.fori_loop(0, 2, piece, 0)

        def g(p, k, so, bo, part=None):
            return G.at[block(k, so, bo, part), lanes(p, k)]

        def add_into(ref, *others):
            def piece(m, carry):
                at = pl.ds(pl.multiple_of(m * 16, 16), 16)
                total = ref[at, :].astype(F32)
                for other in others:
                    total = total + other[at, :].astype(F32)
                ref[at, :] = total.astype(BF)
                return carry
            lax.fori_loop(0, ref.shape[0] // 16, piece, 0)

        def s1(p):
            for j, r in enumerate(ORDER):
                for k in (0, 1):
                    for i, d in enumerate((1, -1)):
                        send(3 + p, ("g1", p, j), g(p, k, r, 2, i), R1[p].at[k, i, j],
                             big_dev(k, d))

        def s2(p, j):
            r = ORDER[j]
            arrived(("g1", p, j), blocks(G, p, 1))
            for k in (0, 1):
                for i, d in enumerate((1, -1)):
                    add_into(g(p, k, r, d, i), R1[p].at[k, i, j])
            for k in (0, 1):
                for i, d in enumerate((1, -1)):
                    send(3 + p, ("g2", p, j), g(p, k, r, d), R2[p].at[k, i, j], big_dev(k, d))

        def two(p, j):
            arrived(("g2", p, j), blocks(G, p, 2))

        def s3(p):
            two(p, 0)
            for k in (0, 1):
                add_into(g(p, k, 2, 0), R2[p].at[k, 0, 0], R2[p].at[k, 1, 0])
            for k in (0, 1):
                for i, d in enumerate((1, -1)):
                    send(3 + p, ("g3", p), g(p, k, 2, 0, i), R3[p].at[k, i], small_dev(k, d))

        def pre4(p):
            for i, d in enumerate((1, -1)):
                two(p, 1 + i)
                for k in (0, 1):
                    add_into(g(p, k, d, 0), R2[p].at[k, 0, 1 + i], R2[p].at[k, 1, 1 + i])

        def s4(p):
            arrived(("g3", p), blocks(G, p, 1))
            for k in (0, 1):
                for i, d in enumerate((1, -1)):
                    add_into(g(p, k, d, 0, i), R3[p].at[k, i])
            for k in (0, 1):
                for i, d in enumerate((1, -1)):
                    send(3 + p, ("g4", p), g(p, k, d, 0), R4[p].at[k, i], small_dev(k, d))

        def keep(p, k, *others):
            own, to = g(p, k, 0, 0), SUM.at[:, lanes(p, k)]

            def piece(m, carry):
                at = pl.ds(pl.multiple_of(m * 16, 16), 16)
                total = own[at, :].astype(F32)
                for other in others:
                    total = total + other[at, :].astype(F32)
                to[at, :] = total
                return carry

            lax.fori_loop(0, rows // 16, piece, 0)

        def partial_of(xo, core):
            start = (turn(x, xo) * 2 + core) * feats
            span = pl.ds(pl.multiple_of(start, feats), feats)

            def piece(m, carry):
                at = pl.ds(pl.multiple_of(m * tile, tile), tile)
                total = 0.0
                for p in (0, 1):
                    lane = slice(base[p], base[p] + 2 * size[p])
                    total = total + dot(D[at, lane], W[span, lane], ((1,), (1,)))
                PD[at, span] = total.astype(BF)
                return carry
            lax.fori_loop(0, 3, piece, 0)

        def pd(xo, core, part=None):
            start = (turn(x, xo) * 2 + core) * feats
            lane = pl.ds(pl.multiple_of(start, feats), feats)
            if part is None:
                return PD.at[:, lane]
            return PD.at[part * halftok : (part + 1) * halftok, lane]

        for o in (0, 1, -1):
            for k in (0, 1):
                forward(0, k, o, o == 0)
        far_arrived(1, 0)
        last_arrived(0)
        for k in (0, 1):
            forward(0, k, 2)
        gate(0)
        far_arrived(1, 1)
        far_arrived(1, -1)
        for k in (0, 1):
            grads(0, k, 2)
        far_arrived(1, 2)
        s1(0)
        for o in (1, -1):
            for k in (0, 1):
                grads(0, k, o)

        for j, o in enumerate((0, 1, -1)):
            for k in (0, 1):
                forward(1, k, o, o == 0)
            s2(0, j)
        last_arrived(1)
        for k in (0, 1):
            forward(1, k, 2)
        gate(1)
        for k in (0, 1):
            grads(1, k, 2)
        s1(1)
        for o in (1, -1):
            for k in (0, 1):
                grads(1, k, o)
        for k in (0, 1):
            grads(0, k, 0)
        s3(0)
        s2(0, 3)
        for j, r in enumerate(ORDER):
            partial_of(r, 1 - c)
            send(5, ("d0", j), pd(r, 1 - c), E0.at[j], sibling)

        def sibling_sum(j):
            arrived(("d0", j), PD.at[:, 0:feats])
            add_into(pd(ORDER[j], c), E0.at[j])

        partial_of(2, c)
        sibling_sum(0)
        for i, d in enumerate((1, -1)):
            send(5, "d1", pd(2, c, i), E1.at[i], x_dev(d))
        for j in (1, 2):
            partial_of(ORDER[j], c)
            sibling_sum(j)
        for j in (0, 1, 2):
            s2(1, j)
        pre4(0)
        partial_of(0, c)
        s4(0)
        arrived("d1", PD.at[:, 0:feats])
        for i, d in enumerate((1, -1)):
            add_into(pd(d, c, i), E1.at[i])
            send(5, "d2", pd(d, c), E2.at[i], x_dev(d))
        for k in (0, 1):
            grads(1, k, 0)
        s3(1)
        s2(1, 3)
        pre4(1)

        stores = []

        def store(src, dst):
            copy = pltpu.make_async_copy(src, dst, store_sem.at[len(stores)])
            copy.start()
            stores.append(copy)

        def finish_dx():
            arrived(("d0", 3), PD.at[:, 0:feats])
            arrived("d2", PD.at[:, 0 : 2 * feats])
            own = pd(0, c)

            def piece(m, carry):
                at = pl.ds(pl.multiple_of(m * 16, 16), 16)
                total = (own[at, :].astype(F32) + E0[3, at, :].astype(F32)
                         + E2[0, at, :].astype(F32) + E2[1, at, :].astype(F32))
                DX[at, :] = total.astype(BF)
                return carry

            lax.fori_loop(0, tokens // 16, piece, 0)
            store(DX, dx_out)

        def finish_grads(p):
            two(p, 3)
            if p == 0:
                arrived(("g4", p), blocks(G, p, 2))
            for k in (0, 1):
                late = [R4[p].at[k, i] for i in (0, 1)] if p == 0 else []
                keep(p, k, R2[p].at[k, 0, 3], R2[p].at[k, 1, 3], *late)
            at = slice(base[p], base[p] + 3 * size[p])
            store(SUM.at[:, at], sum_out.at[:, at])

        finish_dx()
        s4(1)
        finish_grads(0)
        finish_grads(1)
        for p in (0, 1):
            left(p, blocks(W, p, 15))
            left(3 + p, blocks(G, p, 15))
        left(2, XQ.at[:, 0 : 7 * feats])
        left(5, PD.at[:, 0 : 7 * feats])
        for copy in stores:
            copy.wait()
        arrived(("g4", 1), blocks(G, 1, 2))

    count = 2 * (1 + 1 + 4 + 1) + 4 + 2 * (4 + 4 + 1 + 1) + 4 + 1 + 1
    n = [3 * h // 2 for h in size]
    scratch = [
        pltpu.VMEM((width, every), BF),
        pltpu.VMEM((2 * tokens, width), BF),
        pltpu.VMEM((tokens, every), F32),
        pltpu.VMEM((tokens, every), BF),
        pltpu.VMEM((width, every), BF),
        *[pltpu.VMEM((2, 2, SIDE, half, m), BF) for m in n],
        *[pltpu.VMEM((2, 2, SIDE, rows, m), BF) for m in n],
        *[pltpu.VMEM((2, 2, half, m), BF) for m in n],
        pltpu.VMEM((2, 2, rows, n[0]), BF),
        pltpu.VMEM((tokens, width), BF),
        pltpu.VMEM((SIDE, tokens, feats), BF),
        pltpu.VMEM((2, halftok, feats), BF),
        pltpu.VMEM((2, tokens, feats), BF),
        pltpu.VMEM((hidden, rows), BF),
        pltpu.VMEM((rows, every), F32),
        pltpu.VMEM((tokens, feats), BF),
        pltpu.SemaphoreType.DMA((7,)),
        pltpu.SemaphoreType.DMA((3,)),
        pltpu.SemaphoreType.DMA((6,)),
        pltpu.SemaphoreType.DMA((count,)),
    ]
    return kernel, scratch


def finish_of(rows, hidden):
    size, base = shares(hidden)
    n = 3 * size[1] // 2
    cut = n - size[1]

    def finish(dx_in, sum_in, late_in, dx_out, gate_out, up_out, down_out,
               DX, SUM, LATE, UP, GATE, DOWN, ins, outs):
        first = slice(0, base[1])
        last = slice(base[1], base[1] + 3 * size[1])
        loads = [
            pltpu.make_async_copy(sum_in.at[:, first], SUM.at[:, first], ins.at[0]),
            pltpu.make_async_copy(sum_in.at[:, last], SUM.at[:, last], ins.at[1]),
            pltpu.make_async_copy(late_in, LATE, ins.at[2]),
            pltpu.make_async_copy(dx_in, DX, ins.at[3]),
        ]
        for load in loads:
            load.start()
        h = size[0]
        loads[0].wait()
        DOWN[0:h, :] = SUM[:, 2 * h : 3 * h].T
        GATE[:, 0:h] = SUM[:, 0:h]
        UP[:, 0:h] = SUM[:, h : 2 * h]
        for load in loads[1:]:
            load.wait()
        at = base[1]
        total = [SUM[:, at + k * n : at + (k + 1) * n] + LATE[k, 0].astype(F32) + LATE[k, 1].astype(F32)
                 for k in (0, 1)]
        DOWN[h:hidden, :] = total[1][:, cut:n].T
        GATE[:, h:hidden] = total[0][:, 0 : size[1]]
        UP[:, h : h + cut] = total[0][:, size[1] : n]
        UP[:, h + cut : hidden] = total[1][:, 0:cut]
        stores = [
            pltpu.make_async_copy(DX, dx_out, outs.at[0]),
            pltpu.make_async_copy(GATE, gate_out, outs.at[1]),
            pltpu.make_async_copy(UP, up_out, outs.at[2]),
            pltpu.make_async_copy(DOWN, down_out, outs.at[3]),
        ]
        for copy in stores:
            copy.start()
        for copy in stores:
            copy.wait()

    return finish


def solution(mesh):
    def on_device(layer_input, out_cotangent, gate_matrix, up_matrix, down_matrix):
        tokens, feats = layer_input.shape
        rows, hidden = gate_matrix.shape
        width = feats * mesh.shape["tp"]
        kernel, scratch = kernel_of(rows, tokens, width, hidden)
        flops = 2 * 8 * tokens * width * hidden
        late = (2, 2, rows, shares(hidden)[0][1] * 3 // 2)
        any_space = pl.BlockSpec(memory_space=pl.ANY)
        dx, sums, lates = pl.pallas_call(
            kernel,
            out_shape=(
                jax.ShapeDtypeStruct((tokens, feats), BF),
                jax.ShapeDtypeStruct((rows, 3 * hidden), F32),
                jax.ShapeDtypeStruct(late, BF),
            ),
            in_specs=[any_space] * 5,
            out_specs=[any_space] * 3,
            scratch_shapes=scratch,
            compiler_params=pltpu.CompilerParams(
                collective_id=0, has_side_effects=True, vmem_limit_bytes=66_000_000),
            cost_estimate=pl.CostEstimate(
                flops=flops, bytes_accessed=4 << 20, transcendentals=tokens * hidden),
        )(layer_input, out_cotangent, gate_matrix, up_matrix, down_matrix)
        return pl.pallas_call(
            finish_of(rows, hidden),
            out_shape=(
                jax.ShapeDtypeStruct((tokens, feats), BF),
                jax.ShapeDtypeStruct((rows, hidden), F32),
                jax.ShapeDtypeStruct((rows, hidden), F32),
                jax.ShapeDtypeStruct((hidden, rows), F32),
            ),
            in_specs=[any_space] * 3,
            out_specs=[any_space] * 4,
            scratch_shapes=[
                pltpu.VMEM((tokens, feats), BF),
                pltpu.VMEM((rows, 3 * hidden), F32),
                pltpu.VMEM(late, BF),
                pltpu.VMEM((rows, hidden), F32),
                pltpu.VMEM((rows, hidden), F32),
                pltpu.VMEM((hidden, rows), F32),
                pltpu.SemaphoreType.DMA((4,)),
                pltpu.SemaphoreType.DMA((4,)),
            ],
        )(dx, sums, lates)

    return jax.shard_map(
        on_device, mesh=mesh,
        in_specs=(P("fs", "tp"), P("fs", "tp"), P("fs", "tp"), P("fs", "tp"), P("tp", "fs")),
        out_specs=(P("fs", "tp"), P("fs", "tp"), P("fs", "tp"), P("tp", "fs")),
        check_vma=False)
```

time: 303 us -> 109 us (0.36)
  waiting for transfers between devices: 155 us -> 0 us
  Pallas kernels: 0 us -> 108 us
  blocking collectives: 60.7 us -> 0 us
  matrix products: 35.8 us -> 0 us
  local copies, waits for them, and re-layouts: 20.4 us -> 0 us
  other arithmetic: 16.6 us -> 0 us
  between operations: 13.9 us -> 0.64 us
    all_gather x3 -> x0, waiting for transfers between devices: 119 us -> none  [the longest x2 92.1 us: side_by_side(): filled, at, done = (lax.all_gather(both, axis, axis=dim, tiled=True), 0, [])]
    pallas_call x0 -> x2, Pallas kernels: none -> 108 us  [the longest x1 105 us: on_device(): pl.pallas_call(kernel, out_shape=(jax.ShapeDtypeStruct((tokens, feats), B...]
    all_to_all x1 -> x0, blocking collectives: 42.5 us -> none  [summed_on_arrival(): lax.all_to_all(pieces, axis, split_axis=0, concat_axis=0, tiled=True)]
    dot_general x7 -> x0, matrix products: 35.8 us -> none  [the longest x3 15.2 us: outer_cols(): lax.dot_general(left, right, (((1,), (1,)), ((), ())), preferred_element_...]
    unnamed x5 -> x0, waiting for transfers between devices: 35.2 us -> none
    unnamed x26 -> x0, local copies, waits for them, and re-layouts: 19.4 us -> none
    all_gather x1 -> x0, blocking collectives: 18.2 us -> none  [gather_axes(): filled = lax.all_gather(filled, axes[number], axis=dim, tiled=True)]
    concatenate x3 -> x0, other arithmetic: 15.3 us -> none  [the longest x1 11.4 us: on_device(): jnp.concatenate((inner_rows(whole_input, both_delta), inner_rows(whole_co...]
  transfers between devices with their start and end apart: 4 -> 0, of which waited for: 4 -> 0; matrix products, arithmetic and copies ran while one was open for 7% -> 0% of each run, Pallas kernels for 0% -> 0%
where the time goes in v2:
time: 109 us
  Pallas kernels  108 us (99%)
    pallas_call x1, Pallas kernels, on_device(): pl.pallas_call(kernel, out_shape=(jax.ShapeDtypeStruct((tokens, feats), B...  105 us
    pallas_call x1, Pallas kernels, on_device(): pl.pallas_call(finish_of(rows, hidden), out_shape=(jax.ShapeDtypeStruct((...  2.67 us

profile of v2, /device:TPU:0, one launch (start us, length us, event | category | flops | bytes accessed | tf_op | source)
XLA Modules:
  0.0 108.8 jit_solution(3484642405298995631)
XLA Ops:
  0.6 105.5 %shard_map.84 = (bf16[768,256]{1,0:T(8,128)(2,1)}, f32[128,2304]{1,0:T(8,128)}, bf16[2,2,128,384]{3,2,1,0:T(8,128)(2,1)}) custom-call(bf16[768,256]{1,0:T(8,128)(2,1)} %x_in.1, bf16[768,256]{1,0:T(8,128)(2,1)} %q_in.1, bf16[128,768]{1,0:T(8,128)(2,1)} %gate_in.1, bf16[128,768]{1,0:T(8,128)(2,1)} %up_in.1, bf16[768,128]{1,0:T(8,128)(2,1)} %down_in.1), custom_call_target="tpu_custom_call" | custom-call | flops 19327352832 | bytes 4194304 | tf_op jit(solution)/shard_map/pallas_call | solution.py:576
  106.1 2.7 %shard_map.85 = (bf16[768,256]{1,0:T(8,128)(2,1)}, f32[128,768]{1,0:T(8,128)}, f32[128,768]{1,0:T(8,128)}, f32[768,128]{1,0:T(8,128)}) custom-call(bf16[768,256]{1,0:T(8,128)(2,1)} %get-tuple-element.7.dx_in, f32[128,2304]{1,0:T(8,128)} %get-tuple-element.8.sum_in, bf16[2,2,128,384]{3,2,1,0:T(8,128)(2,1)} %get-tuple-element.9.late_in), custom_call_target="tpu_custom_call" | custom-call | tf_op jit(solution)/shard_map/pallas_call | solution.py:591

commit v3 on v2

--- a/solution.py
+++ b/solution.py
@@ -59,30 +59,28 @@
             pl.semaphore_signal(barrier, inc=1, device_id=partner, device_id_type=MESH)
         mine = pl.ds(pl.multiple_of(fs * rows, rows), rows)
         my_feats = pl.ds(pl.multiple_of(tp * feats, feats), feats)
-        loads = [
-            pltpu.make_async_copy(down_in, DN, load_sem.at[0]),
-            pltpu.make_async_copy(x_in, XQ.at[0:tokens, my_feats], load_sem.at[1]),
-            pltpu.make_async_copy(q_in, XQ.at[tokens : 2 * tokens, my_feats], load_sem.at[2]),
-        ]
+        loads = []
+
+        def load(src, dst):
+            copy = pltpu.make_async_copy(src, dst, load_sem.at[len(loads)])
+            copy.start()
+            loads.append(copy)
+
         for p in (0, 1):
             at, h, from_ = base[p], size[p], p * size[0]
             for i, ref in enumerate((gate_in, up_in)):
-                loads.append(pltpu.make_async_copy(
-                    ref.at[:, from_ : from_ + h], W.at[mine, at + i * h : at + (i + 1) * h],
-                    load_sem.at[len(loads)]))
-        for load in loads:
-            load.start()
-
-        def load_in():
-            loads[0].wait()
+                load(ref.at[:, from_ : from_ + h], W.at[mine, at + i * h : at + (i + 1) * h])
+            if p == 0:
+                load(down_in, DN)
+                load(x_in, XQ.at[0:tokens, my_feats])
+                load(q_in, XQ.at[tokens : 2 * tokens, my_feats])
+
+        def turn_down():
+            loads[2].wait()
             turned = DN[...].astype(F32).T.astype(BF)
             for p in (0, 1):
                 at, h, from_ = base[p], size[p], p * size[0]
                 W[mine, at + 2 * h : at + 3 * h] = turned[:, from_ : from_ + h]
-            for load in loads[1:]:
-                load.wait()
-
-        load_in()
 
         def meet():
             pl.semaphore_wait(barrier, 7)
@@ -191,13 +189,20 @@
         def x_last():
             arrived("sib", XQ.at[:, 0 : 4 * feats])
 
+        loads[0].wait()
+        loads[1].wait()
         near(0, 0)
-        x_own(0)
+        turn_down()
         near(0, 1)
         far(0, 0)
+        loads[3].wait()
+        loads[4].wait()
+        x_own(0)
         x_own(1)
         for part in (0, 1):
             to_sibling(0, part)
+        loads[5].wait()
+        loads[6].wait()
         for k in (0, 1):
             near(1, k)
 
@@ -536,28 +541,32 @@
         ]
         for load in loads:
             load.start()
-        h = size[0]
+        h, at = size[0], base[1]
+        stores = []
+
+        def store(src, dst):
+            copy = pltpu.make_async_copy(src, dst, outs.at[len(stores)])
+            copy.start()
+            stores.append(copy)
+
         loads[0].wait()
+        store(SUM.at[:, 0:h], gate_out.at[:, 0:h])
+        store(SUM.at[:, h : 2 * h], up_out.at[:, 0:h])
         DOWN[0:h, :] = SUM[:, 2 * h : 3 * h].T
-        GATE[:, 0:h] = SUM[:, 0:h]
-        UP[:, 0:h] = SUM[:, h : 2 * h]
-        for load in loads[1:]:
-            load.wait()
-        at = base[1]
+        store(DOWN.at[0:h, :], down_out.at[0:h, :])
+        loads[1].wait()
+        loads[2].wait()
         total = [SUM[:, at + k * n : at + (k + 1) * n] + LATE[k, 0].astype(F32) + LATE[k, 1].astype(F32)
                  for k in (0, 1)]
+        GATE[...] = total[0][:, 0 : size[1]]
+        store(GATE, gate_out.at[:, h:hidden])
+        UP[:, 0:cut] = total[0][:, size[1] : n]
+        UP[:, cut : size[1]] = total[1][:, 0:cut]
+        store(UP, up_out.at[:, h:hidden])
         DOWN[h:hidden, :] = total[1][:, cut:n].T
-        GATE[:, h:hidden] = total[0][:, 0 : size[1]]
-        UP[:, h : h + cut] = total[0][:, size[1] : n]
-        UP[:, h + cut : hidden] = total[1][:, 0:cut]
-        stores = [
-            pltpu.make_async_copy(DX, dx_out, outs.at[0]),
-            pltpu.make_async_copy(GATE, gate_out, outs.at[1]),
-            pltpu.make_async_copy(UP, up_out, outs.at[2]),
-            pltpu.make_async_copy(DOWN, down_out, outs.at[3]),
-        ]
-        for copy in stores:
-            copy.start()
+        store(DOWN.at[h:hidden, :], down_out.at[h:hidden, :])
+        loads[3].wait()
+        store(DX, dx_out)
         for copy in stores:
             copy.wait()
 
@@ -602,11 +611,11 @@
                 pltpu.VMEM((tokens, feats), BF),
                 pltpu.VMEM((rows, 3 * hidden), F32),
                 pltpu.VMEM(late, BF),
-                pltpu.VMEM((rows, hidden), F32),
-                pltpu.VMEM((rows, hidden), F32),
+                pltpu.VMEM((rows, shares(hidden)[0][1]), F32),
+                pltpu.VMEM((rows, shares(hidden)[0][1]), F32),
                 pltpu.VMEM((hidden, rows), F32),
                 pltpu.SemaphoreType.DMA((4,)),
-                pltpu.SemaphoreType.DMA((4,)),
+                pltpu.SemaphoreType.DMA((7,)),
             ],
         )(dx, sums, lates)
 

time: 109 us -> 109 us (level)
  no operation moved by 1% of the time
where the time goes in v3:
time: 109 us
  Pallas kernels  108 us (99%)
    pallas_call x1, Pallas kernels, on_device(): pl.pallas_call(kernel, out_shape=(jax.ShapeDtypeStruct((tokens, feats), B...  106 us
    pallas_call x1, Pallas kernels, on_device(): pl.pallas_call(finish_of(rows, hidden), out_shape=(jax.ShapeDtypeStruct((...  2.38 us

profile of v3, /device:TPU:0, one launch (start us, length us, event | category | flops | bytes accessed | tf_op | source)
XLA Modules:
  0.0 108.6 jit_solution(13494939721579071124)
XLA Ops:
  0.6 105.6 %shard_map.84 = (bf16[768,256]{1,0:T(8,128)(2,1)}, f32[128,2304]{1,0:T(8,128)}, bf16[2,2,128,384]{3,2,1,0:T(8,128)(2,1)}) custom-call(bf16[768,256]{1,0:T(8,128)(2,1)} %x_in.1, bf16[768,256]{1,0:T(8,128)(2,1)} %q_in.1, bf16[128,768]{1,0:T(8,128)(2,1)} %gate_in.1, bf16[128,768]{1,0:T(8,128)(2,1)} %up_in.1, bf16[768,128]{1,0:T(8,128)(2,1)} %down_in.1), custom_call_target="tpu_custom_call" | custom-call | flops 19327352832 | bytes 4194304 | tf_op jit(solution)/shard_map/pallas_call | solution.py:585
  106.3 2.4 %shard_map.85 = (bf16[768,256]{1,0:T(8,128)(2,1)}, f32[128,768]{1,0:T(8,128)}, f32[128,768]{1,0:T(8,128)}, f32[768,128]{1,0:T(8,128)}) custom-call(bf16[768,256]{1,0:T(8,128)(2,1)} %get-tuple-element.7.dx_in, f32[128,2304]{1,0:T(8,128)} %get-tuple-element.8.sum_in, bf16[2,2,128,384]{3,2,1,0:T(8,128)(2,1)} %get-tuple-element.9.late_in), custom_call_target="tpu_custom_call" | custom-call | tf_op jit(solution)/shard_map/pallas_call | solution.py:600

commit v4 on v3

--- a/solution.py
+++ b/solution.py
@@ -268,7 +268,7 @@
                 g = ACC[at, one:two]
                 u = ACC[at, two:three]
                 e = ACC[at, three:four]
-                s = jax.nn.sigmoid(g)
+                s = 1.0 / (1.0 + jnp.exp(-g))
                 act = g * s
                 D[at, one:two] = (e * u * s * (1.0 + g * (1.0 - s))).astype(BF)
                 D[at, two:three] = (e * act).astype(BF)

time: 109 us -> 109 us (level)
  no operation moved by 1% of the time
where the time goes in v4:
time: 109 us
  Pallas kernels  108 us (99%)
    pallas_call x1, Pallas kernels, on_device(): pl.pallas_call(kernel, out_shape=(jax.ShapeDtypeStruct((tokens, feats), B...  106 us
    pallas_call x1, Pallas kernels, on_device(): pl.pallas_call(finish_of(rows, hidden), out_shape=(jax.ShapeDtypeStruct((...  2.38 us

profile of v4, /device:TPU:0, one launch (start us, length us, event | category | flops | bytes accessed | tf_op | source)
XLA Modules:
  0.0 108.6 jit_solution(9408853181123643211)
XLA Ops:
  0.6 105.6 %shard_map.84 = (bf16[768,256]{1,0:T(8,128)(2,1)}, f32[128,2304]{1,0:T(8,128)}, bf16[2,2,128,384]{3,2,1,0:T(8,128)(2,1)}) custom-call(bf16[768,256]{1,0:T(8,128)(2,1)} %x_in.1, bf16[768,256]{1,0:T(8,128)(2,1)} %q_in.1, bf16[128,768]{1,0:T(8,128)(2,1)} %gate_in.1, bf16[128,768]{1,0:T(8,128)(2,1)} %up_in.1, bf16[768,128]{1,0:T(8,128)(2,1)} %down_in.1), custom_call_target="tpu_custom_call" | custom-call | flops 19327352832 | bytes 4194304 | tf_op jit(solution)/shard_map/pallas_call | solution.py:585
  106.3 2.4 %shard_map.85 = (bf16[768,256]{1,0:T(8,128)(2,1)}, f32[128,768]{1,0:T(8,128)}, f32[128,768]{1,0:T(8,128)}, f32[768,128]{1,0:T(8,128)}) custom-call(bf16[768,256]{1,0:T(8,128)(2,1)} %get-tuple-element.7.dx_in, f32[128,2304]{1,0:T(8,128)} %get-tuple-element.8.sum_in, bf16[2,2,128,384]{3,2,1,0:T(8,128)(2,1)} %get-tuple-element.9.late_in), custom_call_target="tpu_custom_call" | custom-call | tf_op jit(solution)/shard_map/pallas_call | solution.py:600

commit v5 on v4

--- a/solution.py
+++ b/solution.py
@@ -27,7 +27,7 @@
 
     def kernel(x_in, q_in, gate_in, up_in, down_in, dx_out, sum_out, late_out,
                W, XQ, ACC, D, G, R1a, R1b, R2a, R2b, R3a, R3b, R4a, PD, E0, E1, E2, DN, SUM, DX,
-               load_sem, store_sem, ss, rs):
+               load_sem, ss, rs):
         R1, R2, R3, R4 = (R1a, R1b), (R2a, R2b), (R3a, R3b), (R4a, late_out)
         fs, tp = lax.axis_index("fs"), lax.axis_index("tp")
         z, y = fs // SIDE, fs % SIDE
@@ -87,9 +87,17 @@
 
         meet()
 
-        slots = {}
+        slots, again = {}, {}
+        for p in (0, 1):
+            for j, r in enumerate(ORDER):
+                again["g1", p, j] = "a3", p, r
+            again["g2", p, 0] = "a4", p
+            again["g2", p, 2] = "g2", p, 1
+            again["g3", p] = "a1", p
+            again["g4", p] = "a2", p
 
         def slot(name):
+            name = again.get(name, name)
             if name not in slots:
                 slots[name] = len(slots)
             return slots[name]
@@ -131,18 +139,18 @@
 
         def near(p, k):
             for d in (1, -1):
-                send(p, ("a1", p), w(p, k, 0, 0), w(p, k, 0, 0), small_dev(k, d))
+                send(0, ("a1", p), w(p, k, 0, 0), w(p, k, 0, 0), small_dev(k, d))
 
         def far(p, r):
             for k in (0, 1):
                 for d in (1, -1):
-                    send(p, ("a3", p, r), w(p, k, r, 0), w(p, k, r, 0), big_dev(k, d))
+                    send(0, ("a3", p, r), w(p, k, r, 0), w(p, k, r, 0), big_dev(k, d))
 
         def near_arrived(p):
             arrived(("a1", p), blocks(W, p, 2))
             for k in (0, 1):
                 for i, d in enumerate((1, -1)):
-                    send(p, ("a2", p), w(p, k, -d, 0, i), w(p, k, -d, 0, i), small_dev(k, d))
+                    send(0, ("a2", p), w(p, k, -d, 0, i), w(p, k, -d, 0, i), small_dev(k, d))
 
         def opposite_arrived(p):
             arrived(("a2", p), blocks(W, p, 1))
@@ -151,7 +159,7 @@
             arrived(("a3", p, r), blocks(W, p, 2))
             for k in (0, 1):
                 for i, d in enumerate((1, -1)):
-                    send(p, ("a4", p), w(p, k, r, -d, i), w(p, k, r, -d, i), big_dev(k, d))
+                    send(0, ("a4", p), w(p, k, r, -d, i), w(p, k, r, -d, i), big_dev(k, d))
 
         def last_arrived(p):
             arrived(("a4", p), blocks(W, p, 4))
@@ -313,7 +321,7 @@
             for j, r in enumerate(ORDER):
                 for k in (0, 1):
                     for i, d in enumerate((1, -1)):
-                        send(3 + p, ("g1", p, j), g(p, k, r, 2, i), R1[p].at[k, i, j],
+                        send(1, ("g1", p, j), g(p, k, r, 2, i), R1[p].at[k, i, j],
                              big_dev(k, d))
 
         def s2(p, j):
@@ -324,7 +332,7 @@
                     add_into(g(p, k, r, d, i), R1[p].at[k, i, j])
             for k in (0, 1):
                 for i, d in enumerate((1, -1)):
-                    send(3 + p, ("g2", p, j), g(p, k, r, d), R2[p].at[k, i, j], big_dev(k, d))
+                    send(1, ("g2", p, j), g(p, k, r, d), R2[p].at[k, i, j], big_dev(k, d))
 
         def two(p, j):
             arrived(("g2", p, j), blocks(G, p, 2))
@@ -335,11 +343,11 @@
                 add_into(g(p, k, 2, 0), R2[p].at[k, 0, 0], R2[p].at[k, 1, 0])
             for k in (0, 1):
                 for i, d in enumerate((1, -1)):
-                    send(3 + p, ("g3", p), g(p, k, 2, 0, i), R3[p].at[k, i], small_dev(k, d))
+                    send(1, ("g3", p), g(p, k, 2, 0, i), R3[p].at[k, i], small_dev(k, d))
 
         def pre4(p):
+            arrived(("g2", p, 1), blocks(G, p, 4))
             for i, d in enumerate((1, -1)):
-                two(p, 1 + i)
                 for k in (0, 1):
                     add_into(g(p, k, d, 0), R2[p].at[k, 0, 1 + i], R2[p].at[k, 1, 1 + i])
 
@@ -350,7 +358,7 @@
                     add_into(g(p, k, d, 0, i), R3[p].at[k, i])
             for k in (0, 1):
                 for i, d in enumerate((1, -1)):
-                    send(3 + p, ("g4", p), g(p, k, d, 0), R4[p].at[k, i], small_dev(k, d))
+                    send(1, ("g4", p), g(p, k, d, 0), R4[p].at[k, i], small_dev(k, d))
 
         def keep(p, k, *others):
             own, to = g(p, k, 0, 0), SUM.at[:, lanes(p, k)]
@@ -424,16 +432,16 @@
         s2(0, 3)
         for j, r in enumerate(ORDER):
             partial_of(r, 1 - c)
-            send(5, ("d0", j), pd(r, 1 - c), E0.at[j], sibling)
+            send(3, "d0", pd(r, 1 - c), E0.at[j], sibling)
 
         def sibling_sum(j):
-            arrived(("d0", j), PD.at[:, 0:feats])
             add_into(pd(ORDER[j], c), E0.at[j])
 
         partial_of(2, c)
+        arrived("d0", PD.at[:, 0 : 4 * feats])
         sibling_sum(0)
         for i, d in enumerate((1, -1)):
-            send(5, "d1", pd(2, c, i), E1.at[i], x_dev(d))
+            send(3, "d1", pd(2, c, i), E1.at[i], x_dev(d))
         for j in (1, 2):
             partial_of(ORDER[j], c)
             sibling_sum(j)
@@ -445,7 +453,7 @@
         arrived("d1", PD.at[:, 0:feats])
         for i, d in enumerate((1, -1)):
             add_into(pd(d, c, i), E1.at[i])
-            send(5, "d2", pd(d, c), E2.at[i], x_dev(d))
+            send(3, "d2", pd(d, c), E2.at[i], x_dev(d))
         for k in (0, 1):
             grads(1, k, 0)
         s3(1)
@@ -455,12 +463,11 @@
         stores = []
 
         def store(src, dst):
-            copy = pltpu.make_async_copy(src, dst, store_sem.at[len(stores)])
+            copy = pltpu.make_async_copy(src, dst, load_sem.at[len(stores)])
             copy.start()
             stores.append(copy)
 
         def finish_dx():
-            arrived(("d0", 3), PD.at[:, 0:feats])
             arrived("d2", PD.at[:, 0 : 2 * feats])
             own = pd(0, c)
 
@@ -488,16 +495,15 @@
         s4(1)
         finish_grads(0)
         finish_grads(1)
-        for p in (0, 1):
-            left(p, blocks(W, p, 15))
-            left(3 + p, blocks(G, p, 15))
+        left(0, W.at[0 : 15 * rows, :])
+        left(1, G.at[0 : 15 * rows, :])
         left(2, XQ.at[:, 0 : 7 * feats])
-        left(5, PD.at[:, 0 : 7 * feats])
+        left(3, PD.at[:, 0 : 7 * feats])
         for copy in stores:
             copy.wait()
         arrived(("g4", 1), blocks(G, 1, 2))
 
-    count = 2 * (1 + 1 + 4 + 1) + 4 + 2 * (4 + 4 + 1 + 1) + 4 + 1 + 1
+    count = 2 * (1 + 1 + 4 + 1) + 4 + 2 * 2 + 1 + 1 + 1
     n = [3 * h // 2 for h in size]
     scratch = [
         pltpu.VMEM((width, every), BF),
@@ -517,8 +523,7 @@
         pltpu.VMEM((rows, every), F32),
         pltpu.VMEM((tokens, feats), BF),
         pltpu.SemaphoreType.DMA((7,)),
-        pltpu.SemaphoreType.DMA((3,)),
-        pltpu.SemaphoreType.DMA((6,)),
+        pltpu.SemaphoreType.DMA((4,)),
         pltpu.SemaphoreType.DMA((count,)),
     ]
     return kernel, scratch

time: 109 us -> 108 us (level)
  no operation moved by 1% of the time
where the time goes in v5:
time: 108 us
  Pallas kernels  107 us (99%)
    pallas_call x1, Pallas kernels, on_device(): pl.pallas_call(kernel, out_shape=(jax.ShapeDtypeStruct((tokens, feats), B...  105 us
    pallas_call x1, Pallas kernels, on_device(): pl.pallas_call(finish_of(rows, hidden), out_shape=(jax.ShapeDtypeStruct((...  2.38 us

profile of v5, /device:TPU:0, one launch (start us, length us, event | category | flops | bytes accessed | tf_op | source)
XLA Modules:
  0.0 107.8 jit_solution(12906934192982191598)
XLA Ops:
  0.6 104.8 %shard_map.84 = (bf16[768,256]{1,0:T(8,128)(2,1)}, f32[128,2304]{1,0:T(8,128)}, bf16[2,2,128,384]{3,2,1,0:T(8,128)(2,1)}) custom-call(bf16[768,256]{1,0:T(8,128)(2,1)} %x_in.1, bf16[768,256]{1,0:T(8,128)(2,1)} %q_in.1, bf16[128,768]{1,0:T(8,128)(2,1)} %gate_in.1, bf16[128,768]{1,0:T(8,128)(2,1)} %up_in.1, bf16[768,128]{1,0:T(8,128)(2,1)} %down_in.1), custom_call_target="tpu_custom_call" | custom-call | flops 19327352832 | bytes 4194304 | tf_op jit(solution)/shard_map/pallas_call | solution.py:590
  105.4 2.4 %shard_map.85 = (bf16[768,256]{1,0:T(8,128)(2,1)}, f32[128,768]{1,0:T(8,128)}, f32[128,768]{1,0:T(8,128)}, f32[768,128]{1,0:T(8,128)}) custom-call(bf16[768,256]{1,0:T(8,128)(2,1)} %get-tuple-element.7.dx_in, f32[128,2304]{1,0:T(8,128)} %get-tuple-element.8.sum_in, bf16[2,2,128,384]{3,2,1,0:T(8,128)(2,1)} %get-tuple-element.9.late_in), custom_call_target="tpu_custom_call" | custom-call | tf_op jit(solution)/shard_map/pallas_call | solution.py:605

commit v6 on v5

--- a/solution.py
+++ b/solution.py
@@ -59,24 +59,24 @@
             pl.semaphore_signal(barrier, inc=1, device_id=partner, device_id_type=MESH)
         mine = pl.ds(pl.multiple_of(fs * rows, rows), rows)
         my_feats = pl.ds(pl.multiple_of(tp * feats, feats), feats)
-        loads = []
-
-        def load(src, dst):
-            copy = pltpu.make_async_copy(src, dst, load_sem.at[len(loads)])
-            copy.start()
-            loads.append(copy)
+        def load(group, src, dst):
+            pltpu.make_async_copy(src, dst, load_sem.at[group]).start()
+
+        def loaded(group, like):
+            pltpu.make_async_copy(like, like, load_sem.at[group]).wait()
 
         for p in (0, 1):
             at, h, from_ = base[p], size[p], p * size[0]
             for i, ref in enumerate((gate_in, up_in)):
-                load(ref.at[:, from_ : from_ + h], W.at[mine, at + i * h : at + (i + 1) * h])
+                load(3 * p, ref.at[:, from_ : from_ + h],
+                     W.at[mine, at + i * h : at + (i + 1) * h])
             if p == 0:
-                load(down_in, DN)
-                load(x_in, XQ.at[0:tokens, my_feats])
-                load(q_in, XQ.at[tokens : 2 * tokens, my_feats])
+                load(1, down_in, DN)
+                load(2, x_in, XQ.at[0:tokens, my_feats])
+                load(2, q_in, XQ.at[tokens : 2 * tokens, my_feats])
 
         def turn_down():
-            loads[2].wait()
+            loaded(1, DN)
             turned = DN[...].astype(F32).T.astype(BF)
             for p in (0, 1):
                 at, h, from_ = base[p], size[p], p * size[0]
@@ -95,6 +95,9 @@
             again["g2", p, 2] = "g2", p, 1
             again["g3", p] = "a1", p
             again["g4", p] = "a2", p
+        again["g2", 1, 1] = again["g2", 1, 2] = "a3", 0, ORDER[0]
+        again["g2", 1, 3] = "a3", 0, ORDER[1]
+        again["d0"] = "x1", 0
 
         def slot(name):
             name = again.get(name, name)
@@ -197,20 +200,17 @@
         def x_last():
             arrived("sib", XQ.at[:, 0 : 4 * feats])
 
-        loads[0].wait()
-        loads[1].wait()
+        loaded(0, W.at[mine, 0 : 2 * size[0]])
         near(0, 0)
         turn_down()
         near(0, 1)
         far(0, 0)
-        loads[3].wait()
-        loads[4].wait()
+        loaded(2, XQ.at[:, my_feats])
         x_own(0)
         x_own(1)
         for part in (0, 1):
             to_sibling(0, part)
-        loads[5].wait()
-        loads[6].wait()
+        loaded(3, W.at[mine, base[1] : base[1] + 2 * size[1]])
         for k in (0, 1):
             near(1, k)
 
@@ -430,9 +430,10 @@
             grads(0, k, 0)
         s3(0)
         s2(0, 3)
+        left(2, XQ.at[:, 0 : 7 * feats])
         for j, r in enumerate(ORDER):
             partial_of(r, 1 - c)
-            send(3, "d0", pd(r, 1 - c), E0.at[j], sibling)
+            send(2, "d0", pd(r, 1 - c), E0.at[j], sibling)
 
         def sibling_sum(j):
             add_into(pd(ORDER[j], c), E0.at[j])
@@ -441,7 +442,7 @@
         arrived("d0", PD.at[:, 0 : 4 * feats])
         sibling_sum(0)
         for i, d in enumerate((1, -1)):
-            send(3, "d1", pd(2, c, i), E1.at[i], x_dev(d))
+            send(2, "d1", pd(2, c, i), E1.at[i], x_dev(d))
         for j in (1, 2):
             partial_of(ORDER[j], c)
             sibling_sum(j)
@@ -453,7 +454,7 @@
         arrived("d1", PD.at[:, 0:feats])
         for i, d in enumerate((1, -1)):
             add_into(pd(d, c, i), E1.at[i])
-            send(3, "d2", pd(d, c), E2.at[i], x_dev(d))
+            send(2, "d2", pd(d, c), E2.at[i], x_dev(d))
         for k in (0, 1):
             grads(1, k, 0)
         s3(1)
@@ -491,19 +492,18 @@
             at = slice(base[p], base[p] + 3 * size[p])
             store(SUM.at[:, at], sum_out.at[:, at])
 
+        s4(1)
         finish_dx()
-        s4(1)
         finish_grads(0)
         finish_grads(1)
         left(0, W.at[0 : 15 * rows, :])
         left(1, G.at[0 : 15 * rows, :])
-        left(2, XQ.at[:, 0 : 7 * feats])
-        left(3, PD.at[:, 0 : 7 * feats])
+        left(2, PD.at[:, 0 : 7 * feats])
         for copy in stores:
             copy.wait()
         arrived(("g4", 1), blocks(G, 1, 2))
 
-    count = 2 * (1 + 1 + 4 + 1) + 4 + 2 * 2 + 1 + 1 + 1
+    count = 2 * (1 + 1 + 4 + 1) + 4 + 2 + 1 + 1
     n = [3 * h // 2 for h in size]
     scratch = [
         pltpu.VMEM((width, every), BF),
@@ -522,8 +522,8 @@
         pltpu.VMEM((hidden, rows), BF),
         pltpu.VMEM((rows, every), F32),
         pltpu.VMEM((tokens, feats), BF),
-        pltpu.SemaphoreType.DMA((7,)),
         pltpu.SemaphoreType.DMA((4,)),
+        pltpu.SemaphoreType.DMA((3,)),
         pltpu.SemaphoreType.DMA((count,)),
     ]
     return kernel, scratch
@@ -538,42 +538,39 @@
                DX, SUM, LATE, UP, GATE, DOWN, ins, outs):
         first = slice(0, base[1])
         last = slice(base[1], base[1] + 3 * size[1])
-        loads = [
-            pltpu.make_async_copy(sum_in.at[:, first], SUM.at[:, first], ins.at[0]),
-            pltpu.make_async_copy(sum_in.at[:, last], SUM.at[:, last], ins.at[1]),
-            pltpu.make_async_copy(late_in, LATE, ins.at[2]),
-            pltpu.make_async_copy(dx_in, DX, ins.at[3]),
-        ]
-        for load in loads:
-            load.start()
         h, at = size[0], base[1]
-        stores = []
-
-        def store(src, dst):
-            copy = pltpu.make_async_copy(src, dst, outs.at[len(stores)])
-            copy.start()
-            stores.append(copy)
-
-        loads[0].wait()
-        store(SUM.at[:, 0:h], gate_out.at[:, 0:h])
-        store(SUM.at[:, h : 2 * h], up_out.at[:, 0:h])
+
+        def load(group, src, dst):
+            pltpu.make_async_copy(src, dst, ins.at[group]).start()
+
+        def store(group, src, dst):
+            pltpu.make_async_copy(src, dst, outs.at[group]).start()
+
+        def done(sems, group, like):
+            pltpu.make_async_copy(like, like, sems.at[group]).wait()
+
+        load(0, sum_in.at[:, first], SUM.at[:, first])
+        load(1, sum_in.at[:, last], SUM.at[:, last])
+        load(1, late_in, LATE)
+        load(1, dx_in, DX)
+        done(ins, 0, SUM.at[:, first])
+        store(0, SUM.at[:, 0:h], gate_out.at[:, 0:h])
+        store(0, SUM.at[:, h : 2 * h], up_out.at[:, 0:h])
         DOWN[0:h, :] = SUM[:, 2 * h : 3 * h].T
-        store(DOWN.at[0:h, :], down_out.at[0:h, :])
-        loads[1].wait()
-        loads[2].wait()
+        store(0, DOWN.at[0:h, :], down_out.at[0:h, :])
+        done(ins, 1, SUM)
+        store(1, DX, dx_out)
         total = [SUM[:, at + k * n : at + (k + 1) * n] + LATE[k, 0].astype(F32) + LATE[k, 1].astype(F32)
                  for k in (0, 1)]
         GATE[...] = total[0][:, 0 : size[1]]
-        store(GATE, gate_out.at[:, h:hidden])
+        store(0, GATE, gate_out.at[:, h:hidden])
         UP[:, 0:cut] = total[0][:, size[1] : n]
         UP[:, cut : size[1]] = total[1][:, 0:cut]
-        store(UP, up_out.at[:, h:hidden])
+        store(0, UP, up_out.at[:, h:hidden])
         DOWN[h:hidden, :] = total[1][:, cut:n].T
-        store(DOWN.at[h:hidden, :], down_out.at[h:hidden, :])
-        loads[3].wait()
-        store(DX, dx_out)
-        for copy in stores:
-            copy.wait()
+        store(0, DOWN.at[h:hidden, :], down_out.at[h:hidden, :])
+        done(outs, 1, DX)
+        done(outs, 0, SUM)
 
     return finish
 
@@ -619,8 +616,8 @@
                 pltpu.VMEM((rows, shares(hidden)[0][1]), F32),
                 pltpu.VMEM((rows, shares(hidden)[0][1]), F32),
                 pltpu.VMEM((hidden, rows), F32),
-                pltpu.SemaphoreType.DMA((4,)),
-                pltpu.SemaphoreType.DMA((7,)),
+                pltpu.SemaphoreType.DMA((2,)),
+                pltpu.SemaphoreType.DMA((2,)),
             ],
         )(dx, sums, lates)
 

time: 108 us -> 108 us (level)
  no operation moved by 1% of the time
where the time goes in v6:
time: 108 us
  Pallas kernels  107 us (99%)
    pallas_call x1, Pallas kernels, on_device(): pl.pallas_call(kernel, out_shape=(jax.ShapeDtypeStruct((tokens, feats), B...  105 us
    pallas_call x1, Pallas kernels, on_device(): pl.pallas_call(finish_of(rows, hidden), out_shape=(jax.ShapeDtypeStruct((...  2.37 us

profile of v6, /device:TPU:0, one launch (start us, length us, event | category | flops | bytes accessed | tf_op | source)
XLA Modules:
  0.0 107.7 jit_solution(9439059657341416446)
XLA Ops:
  0.6 104.7 %shard_map.84 = (bf16[768,256]{1,0:T(8,128)(2,1)}, f32[128,2304]{1,0:T(8,128)}, bf16[2,2,128,384]{3,2,1,0:T(8,128)(2,1)}) custom-call(bf16[768,256]{1,0:T(8,128)(2,1)} %x_in.1, bf16[768,256]{1,0:T(8,128)(2,1)} %q_in.1, bf16[128,768]{1,0:T(8,128)(2,1)} %gate_in.1, bf16[128,768]{1,0:T(8,128)(2,1)} %up_in.1, bf16[768,128]{1,0:T(8,128)(2,1)} %down_in.1), custom_call_target="tpu_custom_call" | custom-call | flops 19327352832 | bytes 4194304 | tf_op jit(solution)/shard_map/pallas_call | solution.py:587
  105.3 2.4 %shard_map.85 = (bf16[768,256]{1,0:T(8,128)(2,1)}, f32[128,768]{1,0:T(8,128)}, f32[128,768]{1,0:T(8,128)}, f32[768,128]{1,0:T(8,128)}) custom-call(bf16[768,256]{1,0:T(8,128)(2,1)} %get-tuple-element.7.dx_in, f32[128,2304]{1,0:T(8,128)} %get-tuple-element.8.sum_in, bf16[2,2,128,384]{3,2,1,0:T(8,128)(2,1)} %get-tuple-element.9.late_in), custom_call_target="tpu_custom_call" | custom-call | tf_op jit(solution)/shard_map/pallas_call | solution.py:602

commit v7 on v6

--- a/solution.py
+++ b/solution.py
@@ -317,9 +317,9 @@
                 return carry
             lax.fori_loop(0, ref.shape[0] // 16, piece, 0)
 
-        def s1(p):
+        def s1(p, colours=(0, 1)):
             for j, r in enumerate(ORDER):
-                for k in (0, 1):
+                for k in colours:
                     for i, d in enumerate((1, -1)):
                         send(1, ("g1", p, j), g(p, k, r, 2, i), R1[p].at[k, i, j],
                              big_dev(k, d))
@@ -422,7 +422,7 @@
         gate(1)
         for k in (0, 1):
             grads(1, k, 2)
-        s1(1)
+            s1(1, (k,))
         for o in (1, -1):
             for k in (0, 1):
                 grads(1, k, o)

time: 108 us -> 108 us (level)
  no operation moved by 1% of the time
where the time goes in v7:
time: 108 us
  Pallas kernels  107 us (99%)
    pallas_call x1, Pallas kernels, on_device(): pl.pallas_call(kernel, out_shape=(jax.ShapeDtypeStruct((tokens, feats), B...  105 us
    pallas_call x1, Pallas kernels, on_device(): pl.pallas_call(finish_of(rows, hidden), out_shape=(jax.ShapeDtypeStruct((...  2.37 us

profile of v7, /device:TPU:0, one launch (start us, length us, event | category | flops | bytes accessed | tf_op | source)
XLA Modules:
  0.0 107.7 jit_solution(519032897314043039)
XLA Ops:
  0.6 104.7 %shard_map.84 = (bf16[768,256]{1,0:T(8,128)(2,1)}, f32[128,2304]{1,0:T(8,128)}, bf16[2,2,128,384]{3,2,1,0:T(8,128)(2,1)}) custom-call(bf16[768,256]{1,0:T(8,128)(2,1)} %x_in.1, bf16[768,256]{1,0:T(8,128)(2,1)} %q_in.1, bf16[128,768]{1,0:T(8,128)(2,1)} %gate_in.1, bf16[128,768]{1,0:T(8,128)(2,1)} %up_in.1, bf16[768,128]{1,0:T(8,128)(2,1)} %down_in.1), custom_call_target="tpu_custom_call" | custom-call | flops 19327352832 | bytes 4194304 | tf_op jit(solution)/shard_map/pallas_call | solution.py:587
  105.4 2.4 %shard_map.85 = (bf16[768,256]{1,0:T(8,128)(2,1)}, f32[128,768]{1,0:T(8,128)}, f32[128,768]{1,0:T(8,128)}, f32[768,128]{1,0:T(8,128)}) custom-call(bf16[768,256]{1,0:T(8,128)(2,1)} %get-tuple-element.7.dx_in, f32[128,2304]{1,0:T(8,128)} %get-tuple-element.8.sum_in, bf16[2,2,128,384]{3,2,1,0:T(8,128)(2,1)} %get-tuple-element.9.late_in), custom_call_target="tpu_custom_call" | custom-call | tf_op jit(solution)/shard_map/pallas_call | solution.py:602
